TPU v7x, 32 devices: a whole 2x2x4 slice. The times are simulated.
32 devices in a mesh: ep: 4 (over y, x), tp: 8 (over z, core).
Axes of the slice: x: 2, y: 2, z: 4, core: 2. Of those that a mesh axis runs over, the one named last changes fastest.
Arguments:
- queries: bfloat16 [2048, 16, 128], P('ep', 'tp'), may hold values from -125 to 125
- keys: bfloat16 [2048, 16, 128], P('ep', 'tp'), may hold values from -9 to 9
- values: bfloat16 [2048, 16, 128], P('ep', 'tp'), may hold values from -6 to 6
- mixing: float32 [16], P('tp'), may hold values from 0.3 to 0.8
- head_gain: float32 [128], replicated, may hold values from 0.1 to 1.9
- out_weight: bfloat16 [16, 128, 2048], P('tp'), may hold values from -0.125 to 0.125
- tokens_b: bfloat16 [4096, 2048], P(('ep', 'tp')), may hold values from -6 to 6
- norm_gain: float32 [2048], replicated, may hold values from 0.1 to 1.9
- expert_ids: int32 [4096, 2], P(('ep', 'tp')), may hold values from 0 to 3, all different within a row; in each aligned block of 128 rows (0 to 127, 128 to 255, ...) at most 96 rows name the same one
- group_gate: float32 [4096], P(('ep', 'tp')), may hold values from 0.2 to 1
- expert_gate: float32 [4096, 2], P(('ep', 'tp')), may hold values from 0.1 to 0.9
- gate_weight: bfloat16 [4, 2048, 1024], P('ep', None, 'tp'), may hold values from -0.125 to 0.125
- up_weight: bfloat16 [4, 2048, 1024], P('ep', None, 'tp'), may hold values from -0.125 to 0.125
- down_weight: bfloat16 [4, 2048, 1024], P('ep', None, 'tp'), may hold values from -0.1875 to 0.1875
Outputs:
- mixed: bfloat16 [2048, 2048], P(('ep', 'tp'))
- routed: bfloat16 [4096, 2048], P(('ep', 'tp'))
Inputs may be any that keep to these rules, and one draw needn't show every extreme that they name: `expert_ids`: within each aligned block of 128 rows, no expert is named by more than 96 rows, and some block has an expert named by exactly 96 rows.
All inputs are finite; a program needn't handle non-finite values.
Results may differ from a plain program's by a relative error of at most 0.019.
Values may be sent and summed in bfloat16 or wider, within the bound.
A program may use at most 192 MiB of HBM per device.

v0:
```python
import functools
import math

import jax
import jax.numpy as jnp
from jax import lax
from jax.experimental import pallas as pl
from jax.experimental.pallas import tpu as pltpu
from jax.sharding import PartitionSpec as P

HEAD = 64
CHUNKS = 4
F32 = jnp.float32
BF16 = jnp.bfloat16
MESH = pl.DeviceIdType.MESH
NT = (((1,), (1,)), ((), ()))


def kernel(
    ep,
    tp,
    mix_ref,
    q_ref,
    kv_ref,
    gain_ref,
    ow_ref,
    tok_ref,
    norm_ref,
    ids_ref,
    group_ref,
    gates_ref,
    gate_ref,
    up_ref,
    dn_ref,
    mixed_ref,
    routed_ref,
    kv_all,
    w_gu,
    w_dn,
    rows_x,
    acc,
    hid,
    give,
    take,
    back,
    ret,
    att,
    part,
    pair,
    chip_sum,
    landed,
    line_out,
    out_ref,
    place_ref,
    route_ref,
    local_sem,
    kv_s,
    kv_r,
    x_s,
    x_r,
    xp_s,
    xp_r,
    gu_s,
    gu_r,
    dn_s,
    dn_r,
    pr_s,
    pr_r,
    rs_s,
    rs_r,
    o_s,
    o_r,
    b_s,
    b_r,
):
    chips = tp // 2
    me = lax.axis_index("ep")
    mine = lax.axis_index("tp")
    z = mine // 2
    core = mine % 2
    other = z * 2 + 1 - core
    heads, length, wide = q_ref.shape
    cap = out_ref.shape[1]
    half = ep * cap
    unit = dn_ref.shape[2]
    step = dn_ref.shape[1]
    joined = gate_ref.shape[1] != unit

    def remote(src, dst, send, recv, target):
        return pltpu.make_async_remote_copy(
            src_ref=src,
            dst_ref=dst,
            send_sem=send,
            recv_sem=recv,
            device_id=target,
            device_id_type=MESH,
        )

    barrier = pltpu.get_barrier_semaphore()
    for s in range(1, ep):
        pl.semaphore_signal(
            barrier, inc=1, device_id={"ep": (me + s) % ep}, device_id_type=MESH
        )
    for s in range(1, tp):
        pl.semaphore_signal(
            barrier, inc=1, device_id={"tp": (mine + s) % tp}, device_id_type=MESH
        )
    pl.semaphore_wait(barrier, ep + tp - 2)

    def gu_copy(src, side):
        target = (z + 1 - 2 * side) * 2 + core
        return remote(
            w_gu.at[src], w_gu.at[src], gu_s.at[side, src], gu_r.at[src], {"tp": target}
        )

    def dn_copy(src, c, side):
        target = (z + 1 - 2 * side) * 2 + core
        return remote(
            w_dn.at[src, c],
            w_dn.at[src, c],
            dn_s.at[side, src, c],
            dn_r.at[src, c],
            {"tp": target},
        )

    def has_next(side):
        return (z < chips - 1) if side == 0 else (z > 0)

    def source(k, side):
        return z - k if side == 0 else z + k

    def exists(k, side):
        return (z >= k) if side == 0 else (z + k <= chips - 1)

    own = [
        pltpu.make_async_copy(
            gate_ref, w_gu.at[z] if joined else w_gu.at[z, :, pl.ds(0, unit)], local_sem.at[0]
        ),
        pltpu.make_async_copy(dn_ref, w_dn.at[z], local_sem.at[1]),
        pltpu.make_async_copy(kv_ref, kv_all.at[0], local_sem.at[2]),
        pltpu.make_async_copy(out_ref.at[0], rows_x.at[pl.ds(0, cap)], local_sem.at[3]),
    ]
    if not joined:
        own.append(
            pltpu.make_async_copy(up_ref, w_gu.at[z, :, pl.ds(unit, unit)], local_sem.at[4])
        )
    for copy in own[:3] + own[4:]:
        copy.start()

    def kv_copy(s):
        return remote(kv_ref, kv_all.at[s], kv_s.at[s], kv_r.at[s], {"ep": lax.rem(me + s, ep)})

    for s in range(1, ep):
        pl.when(me + s < ep)(lambda s=s: kv_copy(s).start())
    own[0].wait()
    if not joined:
        own[4].wait()
    for side in range(2):
        pl.when(has_next(side))(lambda side=side: gu_copy(z, side).start())
    own[1].wait()
    for side in range(2):

        @pl.when(has_next(side))
        def _(side=side):
            for c in range(CHUNKS):
                dn_copy(z, c, side).start()

    def x_copy(s):
        return remote(
            out_ref.at[s],
            rows_x.at[pl.ds(s * cap, cap)],
            x_s.at[s],
            x_r.at[s],
            {"ep": lax.rem(me + s, ep)},
        )

    def xp_copy(s):
        src = rows_x.at[pl.ds(s * cap, cap)]
        dst = rows_x.at[pl.ds(half + s * cap, cap)]
        return remote(src, dst, xp_s.at[s], xp_r.at[s], {"tp": other})

    def pass_gu(k):
        for side in range(2):

            @pl.when(exists(k, side) & has_next(side))
            def _(side=side):
                src = source(k, side)
                gu_copy(src, side).wait_recv()
                gu_copy(src, side).start()

    def pass_dn(k, c):
        for side in range(2):

            @pl.when(exists(k, side) & has_next(side))
            def _(side=side):
                src = source(k, side)
                dn_copy(src, c, side).wait_recv()
                dn_copy(src, c, side).start()

    tokens = tok_ref[...].astype(F32)
    normed = (
        tokens
        * lax.rsqrt(jnp.mean(tokens * tokens, axis=1, keepdims=True) + 1e-06)
        * norm_ref[...]
    ).astype(BF16)
    local_rows = tok_ref.shape[0]
    relative = ids_ref[...] - me
    relative = jnp.where(relative < 0, relative + ep, relative)
    expert_lane = lax.broadcasted_iota(jnp.int32, (local_rows, ep), 1)
    named = jnp.zeros((local_rows, ep), F32)
    route = jnp.zeros((local_rows, ep), F32)
    for k in range(ids_ref.shape[1]):
        hit = expert_lane == relative[:, k : k + 1]
        named = jnp.where(hit, 1.0, named)
        route = route + jnp.where(hit, group_ref[...] * gates_ref[:, k : k + 1], 0.0)
    route_ref[...] = route
    square = (local_rows, local_rows)
    before = jnp.where(
        lax.broadcasted_iota(jnp.int32, square, 1) < lax.broadcasted_iota(jnp.int32, square, 0),
        1.0,
        0.0,
    ).astype(BF16)
    rank = jnp.dot(before, named.astype(BF16), preferred_element_type=F32)
    rank = jnp.where(named > 0.5, rank, -1.0).astype(jnp.int32)
    slot_lane = lax.broadcasted_iota(jnp.int32, (local_rows, cap), 1)
    for s in list(range(1, ep)) + [0]:
        place = jnp.where(rank[:, s : s + 1] == slot_lane, 1.0, 0.0).astype(BF16)
        place_ref[s] = place
        out_ref[s] = lax.dot_general(
            place, normed, (((0,), (0,)), ((), ())), preferred_element_type=F32
        ).astype(BF16)
        if s:
            x_copy(s).start()
    own[3].start()
    own[3].wait()
    xp_copy(0).start()

    own[2].wait()
    for s in range(1, ep):
        pl.when(me >= s)(lambda s=s: kv_copy(s).wait_recv())
    if chips > 2:
        pass_gu(1)
    tile = min(256, length)
    tiles = length // tile

    def attend(index, carry):
        h = index // tiles
        start = pl.multiple_of((index % tiles) * tile, tile)
        q = q_ref[h, pl.ds(start, tile), :]
        lane = lax.broadcasted_iota(jnp.int32, (tile, wide), 1)
        ratio = []
        for m in range(2):
            pick = (lane < HEAD) if m == 0 else (lane >= HEAD)
            q_map = jnp.where(pick, q, jnp.zeros_like(q))

            def visit(s, state, diagonal=False, q_map=q_map):
                top, total, value = state
                scores = lax.dot_general(
                    q_map, kv_all[s, h, :, :wide], NT, preferred_element_type=F32
                )
                if diagonal:
                    row = start + lax.broadcasted_iota(jnp.int32, scores.shape, 0)
                    col = lax.broadcasted_iota(jnp.int32, scores.shape, 1)
                    scores = jnp.where(col <= row, scores, -1e30)
                fresh = jnp.maximum(top, jnp.max(scores, axis=1, keepdims=True))
                shrink = jnp.exp(top - fresh)
                expo = jnp.exp(scores - fresh)
                total = total * shrink + jnp.sum(expo, axis=1, keepdims=True)
                value = value * shrink + jnp.dot(
                    expo.astype(BF16), kv_all[s, h, :, wide:], preferred_element_type=F32
                )
                return fresh, total, value

            state = (
                jnp.full((tile, 1), -1e30, F32),
                jnp.zeros((tile, 1), F32),
                jnp.zeros((tile, kv_ref.shape[2] - wide), F32),
            )
            state = visit(0, state, True)
            state = lax.fori_loop(1, me + 1, visit, state)
            ratio.append(state[2] / state[1])
        diff = ratio[0] - mix_ref[h] * ratio[1]
        scaled = diff * lax.rsqrt(jnp.mean(diff * diff, axis=1, keepdims=True) + 1e-05)
        att[h, pl.ds(start, tile), :] = (scaled * gain_ref[...]).astype(BF16)
        return carry

    lax.fori_loop(0, heads * tiles, attend, 0)

    block = length // tp

    def project(t, carry):
        rows = pl.ds(pl.multiple_of(t * 2 * block, 2 * block), 2 * block)
        total = 0.0
        for h in range(heads):
            total = total + jnp.dot(att[h, rows, :], ow_ref[h], preferred_element_type=F32)
        part[0, t] = total[:block].astype(BF16)
        part[1, t] = total[block:].astype(BF16)
        return carry

    lax.fori_loop(0, chips, project, 0)
    pair_copy = remote(part.at[1 - core], pair, pr_s, pr_r, {"tp": other})
    pair_copy.start()
    for s in range(1, ep):
        x_copy(s).wait_recv()
        xp_copy(s).start()
    pair_copy.wait_recv()

    def add_pair(t, carry):
        chip_sum[t] = (part[core, t].astype(F32) + pair[t].astype(F32)).astype(BF16)
        return carry

    lax.fori_loop(0, chips, add_pair, 0)

    def line_copy(side, t, first):
        return remote(
            chip_sum.at[t] if first else line_out.at[side, t],
            landed.at[side, t],
            rs_s.at[side, t],
            rs_r.at[side, t],
            {"tp": (z + 1 - 2 * side) * 2 + core},
        )

    def stage_each(k, do):
        for side in range(2):
            at = k if side == 0 else chips - 1 - k
            targets = range(chips - 1, k, -1) if side == 0 else range(chips - 1 - k)

            @pl.when(z == at)
            def _(side=side, targets=targets):
                for t in targets:
                    do(side, t, k == 0)

    def stage_send(side, t, first):
        copy = line_copy(side, t, first)
        if not first:
            copy.wait_recv()
            line_out[side, t] = (
                chip_sum[t].astype(F32) + landed[side, t].astype(F32)
            ).astype(BF16)
        copy.start()

    stage_each(0, stage_send)

    m_tile = 256 if (2 * half) % 256 == 0 else cap
    m_count = 2 * half // m_tile

    def hidden_of(src):
        def one(t, carry):
            rows = pl.ds(pl.multiple_of(t * m_tile, m_tile), m_tile)
            product = jnp.dot(rows_x[rows, :], w_gu[src], preferred_element_type=F32)
            gate = product[:, :unit]
            hid[src, rows, :] = (
                gate / (1.0 + jnp.exp(-gate)) * product[:, unit:]
            ).astype(BF16)
            return carry

        lax.fori_loop(0, m_count, one, 0)

    def down_of(src, c, first=False):
        def one(t, carry):
            rows = pl.ds(pl.multiple_of(t * m_tile, m_tile), m_tile)
            product = lax.dot_general(
                hid[src, rows, :], w_dn[src, c], NT, preferred_element_type=F32
            )
            if first:
                acc[c, rows, :] = product
            else:
                acc[c, rows, :] += product
            return carry

        lax.fori_loop(0, m_count, one, 0)

    def use_gu(k):
        for side in range(2):

            @pl.when(exists(k, side))
            def _(side=side):
                src = source(k, side)
                pl.when(jnp.logical_not(has_next(side)))(lambda: gu_copy(src, side).wait_recv())
                hidden_of(src)

    def use_dn(k, c):
        for side in range(2):

            @pl.when(exists(k, side))
            def _(side=side):
                src = source(k, side)
                pl.when(jnp.logical_not(has_next(side)))(
                    lambda: dn_copy(src, c, side).wait_recv()
                )
                down_of(src, c)

    last = chips - 1
    late = [k for k in (last - 2, last - 1) if k >= 1]
    for s in range(ep):
        xp_copy(s).wait_recv()
    hidden_of(z)
    for c in range(CHUNKS):
        down_of(z, c, True)
    for k in range(1, last):
        if k + 1 < last:
            pass_gu(k + 1)
        use_gu(k)
        if k < last - 2:
            for c in range(CHUNKS):
                pass_dn(k, c)
        elif k == late[0]:
            for c in range(CHUNKS):
                for near in late:
                    pass_dn(near, c)
        stage_each(k, stage_send)
        if k < last - 1:
            for c in range(CHUNKS):
                use_dn(k, c)
    if last > 0:
        use_gu(last)

    def give_copy(c):
        return remote(give.at[c], take.at[c], o_s.at[c], o_r.at[c], {"tp": other})

    def back_copy(c, s):
        return remote(
            back.at[c, s],
            ret.at[c, s],
            b_s.at[c, s],
            b_r.at[c, s],
            {"ep": lax.rem(me + ep - s, ep)},
        )

    def combine(c):
        total = 0.0
        for s in range(ep):
            if s == 0:
                block_rows = back[c, 0]
            else:
                back_copy(c, s).wait_recv()
                block_rows = ret[c, s]
            picked = jnp.dot(place_ref[s], block_rows, preferred_element_type=F32)
            total = total + route_ref[:, s : s + 1] * picked
        routed_ref[:, c * step : (c + 1) * step] = total.astype(BF16)

    for c in range(CHUNKS):
        for k in range(max(last - 1, 1), last + 1):
            use_dn(k, c)
        give[c] = acc[c, half:, :].astype(BF16)
        give_copy(c).start()
        give_copy(c).wait_recv()
        for s in range(ep):
            rows = slice(s * cap, (s + 1) * cap)
            back[c, s] = (acc[c, rows, :] + take[c, rows, :].astype(F32)).astype(BF16)
        for s in range(1, ep):
            back_copy(c, s).start()
        if c > 1:
            combine(c - 2)
    mixed_ref[...] = chip_sum[z]
    for side in range(2):

        @pl.when((z > 0) if side == 0 else (z < chips - 1))
        def _(side=side):
            line_copy(side, z, False).wait_recv()
            mixed_ref[...] = (
                mixed_ref[...].astype(F32) + landed[side, z].astype(F32)
            ).astype(BF16)

    for c in range(max(CHUNKS - 2, 0), CHUNKS):
        combine(c)

    for s in range(1, ep):
        pl.when(me + s < ep)(lambda s=s: kv_copy(s).wait_send())
        x_copy(s).wait_send()
    for s in range(ep):
        xp_copy(s).wait_send()
    for k in range(chips - 1):
        for side in range(2):

            @pl.when(exists(k, side) & has_next(side))
            def _(side=side, k=k):
                src = source(k, side)
                gu_copy(src, side).wait_send()
                for c in range(CHUNKS):
                    dn_copy(src, c, side).wait_send()

    pair_copy.wait_send()
    for k in range(chips - 1):
        stage_each(k, lambda side, t, first: line_copy(side, t, first).wait_send())
    for c in range(CHUNKS):
        give_copy(c).wait_send()
        for s in range(1, ep):
            back_copy(c, s).wait_send()


def per_device(
    queries,
    keys,
    values,
    mixing,
    head_gain,
    out_weight,
    tokens_b,
    norm_gain,
    expert_ids,
    group_gate,
    expert_gate,
    gate_weight,
    up_weight,
    down_weight,
):
    ep = lax.axis_size("ep")
    tp = lax.axis_size("tp")
    chips = tp // 2
    length, heads, wide = queries.shape
    val = values.shape[2]
    local_rows, width = tokens_b.shape
    top_count = expert_ids.shape[1]
    unit = gate_weight.shape[2]
    assert gate_weight.shape[0] == 1 and wide == 2 * HEAD
    capacity = 3 * local_rows * top_count // (2 * ep)
    cap = -(-capacity // 16) * 16
    step = width // CHUNKS

    scaled = (queries.astype(F32) * (1.0 / math.sqrt(HEAD))).astype(BF16).transpose(1, 0, 2)
    kv = jnp.concatenate([keys, values], axis=2).transpose(1, 0, 2)
    gate, up = gate_weight[0], up_weight[0]
    if unit % 128:
        gate = jnp.concatenate([gate, up], axis=1)
    half = ep * cap
    block = length // tp
    vmem = pl.BlockSpec(memory_space=pltpu.VMEM)
    dma = pltpu.SemaphoreType.DMA
    return pl.pallas_call(
        functools.partial(kernel, ep, tp),
        out_shape=(
            jax.ShapeDtypeStruct((block, width), BF16),
            jax.ShapeDtypeStruct((local_rows, width), BF16),
        ),
        in_specs=[pl.BlockSpec(memory_space=pltpu.SMEM)] + [vmem] * 12,
        out_specs=(vmem, vmem),
        scratch_shapes=[
            pltpu.VMEM((ep, heads, length, wide + val), BF16),
            pltpu.VMEM((chips, width, 2 * unit), BF16),
            pltpu.VMEM((chips, CHUNKS, step, unit), BF16),
            pltpu.VMEM((2 * half, width), BF16),
            pltpu.VMEM((CHUNKS, 2 * half, step), F32),
            pltpu.VMEM((chips, 2 * half, unit), BF16),
            pltpu.VMEM((CHUNKS, half, step), BF16),
            pltpu.VMEM((CHUNKS, half, step), BF16),
            pltpu.VMEM((CHUNKS, ep, cap, step), BF16),
            pltpu.VMEM((CHUNKS, ep, cap, step), BF16),
            pltpu.VMEM((heads, length, val), BF16),
            pltpu.VMEM((2, chips, block, width), BF16),
            pltpu.VMEM((chips, block, width), BF16),
            pltpu.VMEM((chips, block, width), BF16),
            pltpu.VMEM((2, chips, block, width), BF16),
            pltpu.VMEM((2, chips, block, width), BF16),
            pltpu.VMEM((ep, cap, width), BF16),
            pltpu.VMEM((ep, local_rows, cap), BF16),
            pltpu.VMEM((local_rows, ep), F32),
            dma((5,)),
            dma((ep,)),
            dma((ep,)),
            dma((ep,)),
            dma((ep,)),
            dma((ep,)),
            dma((ep,)),
            dma((2, chips)),
            dma((chips,)),
            dma((2, chips, CHUNKS)),
            dma((chips, CHUNKS)),
            dma,
            dma,
            dma((2, chips)),
            dma((2, chips)),
            dma((CHUNKS,)),
            dma((CHUNKS,)),
            dma((CHUNKS, ep)),
            dma((CHUNKS, ep)),
        ],
        compiler_params=pltpu.CompilerParams(
            collective_id=0, has_side_effects=True, vmem_limit_bytes=62 * 1024 * 1024
        ),
    )(
        mixing,
        scaled,
        kv,
        head_gain[None],
        out_weight,
        tokens_b,
        norm_gain[None],
        expert_ids,
        group_gate[:, None],
        expert_gate,
        gate,
        up,
        down_weight[0].reshape(CHUNKS, step, unit),
    )


def solution(mesh):
    placed = (
        P("ep", "tp", None),
        P("ep", "tp", None),
        P("ep", "tp", None),
        P("tp"),
        P(),
        P("tp", None, None),
        P(("ep", "tp"), None),
        P(),
        P(("ep", "tp"), None),
        P(("ep", "tp")),
        P(("ep", "tp"), None),
        P("ep", None, "tp"),
        P("ep", None, "tp"),
        P("ep", None, "tp"),
    )
    return jax.shard_map(
        per_device,
        mesh=mesh,
        in_specs=placed,
        out_specs=(P(("ep", "tp"), None), P(("ep", "tp"), None)),
        check_vma=False,
    )
```

profile of v0, /device:TPU:0, one launch (start us, length us, event | category | flops | bytes accessed | tf_op | source)
XLA Modules:
  0.0 132.5 jit_solution(4799795827914490443)
XLA Ops:
  0.6 0.0 copy-start.3
  0.6 0.7 copy-done.3
  1.3 0.0 copy-start.5
  1.3 0.7 copy.19.ids_ref
  2.0 0.0 copy-done.5
  2.0 0.0 copy-start.4
  2.0 0.7 copy.20.group_ref
  2.8 0.0 copy-done.4
  2.8 0.7 copy.21.gates_ref
  3.5 0.0 copy-start.1
  3.5 1.7 %fusion.q_ref = bf16[2,512,128]{2,1,0:T(8,128)(2,1)} fusion(bf16[512,2,128]{2,1,0:T(2,128)(2,1)} %param.14), kind=kLoop, calls=%fused_computation.2 | loop fusion | flops 393216 | bytes 524288 | tf_op jit(solution)/shard_map/transpose | solution.py:521
  5.3 0.0 copy-done.1
  5.3 0.0 copy-start.2
  5.3 0.9 copy-done.2
  6.3 0.9 maximum_bitcast_fusion.kv_ref
  7.1 122.9 %shard_map.149 = (bf16[64,2048]{1,0:T(8,128)(2,1)}, bf16[128,2048]{1,0:T(8,128)(2,1)}) custom-call(f32[2]{0:T(128)} %mix_ref.1, bf16[2,512,128]{2,1,0:T(8,128)(2,1)} %fusion.q_ref, bf16[2,512,256]{2,1,0:T(8,128)(2,1)} %maximum_bitcast_fusion.kv_ref, f32[1,128]{1,0:T(1,128)} %bitcast.15, bf16[2,128,2048]{2,1,0:T(8,128)(2,1)} %ow_ref.1, ...), custom_call_target="tpu_custom_call" | custom-call | tf_op jit(solution)/shard_map/pallas_call | solution.py:530
  130.0 0.0 copy-start
  130.0 1.7 %copy.25 = bf16[64,2048]{1,0:T(8,128)(2,1)} copy(bf16[64,2048]{1,0:T(8,128)(2,1)} %get-tuple-element.4) | data formatting | bytes 524288
  131.7 0.0 copy-done
  131.7 0.8 copy.26
  (2 shorter events, 0.1 us)
Async XLA Ops:
  0.6 0.7 copy-start.3
  1.3 0.7 copy-start.5
  2.0 0.7 copy-start.4
  3.5 1.8 %copy-start.1 = (bf16[512,2,128]{2,1,0:T(2,128)(2,1)S(1)}, bf16[512,2,128]{2,1,0:T(2,128)(2,1)}, u32[]{:S(2)}) copy-start(bf16[512,2,128]{2,1,0:T(2,128)(2,1)} %param.15) | copy-start | bytes 786436
  5.3 1.0 copy-start.2
  130.0 1.7 %copy-start = (bf16[128,2048]{1,0:T(8,128)(2,1)S(1)}, bf16[128,2048]{1,0:T(8,128)(2,1)}, u32[]{:S(2)}) copy-start(bf16[128,2048]{1,0:T(8,128)(2,1)} %get-tuple-element.5) | copy-start | bytes 1572868
where the time goes:
time: 133 us
  Pallas kernels  123 us (92%)
  local copies, waits for them, and re-layouts  6.4 us (5%)
  other arithmetic  2.6 us (2%)
    pallas_call x1, Pallas kernels, per_device(): pl.pallas_call(functools.partial(kernel, ep, tp), out_shape=(jax.ShapeDty...  123 us
    unnamed x18, local copies, waits for them, and re-layouts  5.65 us

commit v1 on v0

v1 whole, which is shorter than its diff:
```python
import functools
import math

import jax
import jax.numpy as jnp
from jax import lax
from jax.experimental import pallas as pl
from jax.experimental.pallas import tpu as pltpu
from jax.sharding import PartitionSpec as P

HEAD = 64
CHUNKS = 4
PIECES = 2
RANKS = 16
F32 = jnp.float32
BF16 = jnp.bfloat16
MESH = pl.DeviceIdType.MESH
NT = (((1,), (1,)), ((), ()))
TN = (((0,), (0,)), ((), ()))


def kernel(
    ep,
    tp,
    mix_ref,
    q_ref,
    kv_ref,
    gain_ref,
    ow_ref,
    tok_ref,
    norm_ref,
    ids_ref,
    group_ref,
    gates_ref,
    gate_ref,
    up_ref,
    dn_ref,
    mixed_ref,
    routed_ref,
    kv_all,
    w_gu,
    w_dn,
    rows_x,
    out_ref,
    nrm,
    rank_ref,
    hid,
    back,
    ret,
    top_ref,
    sum_ref,
    val_ref,
    att,
    part,
    pair,
    chip_sum,
    landed,
    line_out,
    place_ref,
    route_ref,
    local_sem,
    kv_s,
    kv_r,
    t_s,
    t_r,
    x_s,
    x_r,
    gu_s,
    gu_r,
    sg_s,
    sg_r,
    dn_s,
    dn_r,
    sd_s,
    sd_r,
    h_s,
    h_r,
    pr_s,
    pr_r,
    rs_s,
    rs_r,
    b_s,
    b_r,
):
    chips = tp // 2
    me = lax.axis_index("ep")
    mine = lax.axis_index("tp")
    z = mine // 2
    core = mine % 2
    other = z * 2 + 1 - core
    inward = 1 - 2 * (z // (chips // 2))
    heads, length, wide = q_ref.shape
    local_rows, width = tok_ref.shape
    half = rows_x.shape[0] // 2
    cap = half // ep
    step = w_dn.shape[3]
    lanes = w_gu.shape[2] // 2
    unit = lanes // 2
    subs = w_dn.shape[1]
    deep = width // PIECES
    joined = gate_ref.shape[1] != unit
    inner = (z >= 1) & (z <= chips - 2)
    is_end = (z == 0) | (z == chips - 1)
    has_guest = (z == 1) | (z == chips - 2)

    def remote(src, dst, send, recv, target):
        return pltpu.make_async_remote_copy(
            src_ref=src,
            dst_ref=dst,
            send_sem=send,
            recv_sem=recv,
            device_id=target,
            device_id_type=MESH,
        )

    if joined:
        own_gu = [pltpu.make_async_copy(gate_ref, w_gu.at[z, :, pl.ds(0, lanes)], local_sem.at[0])]
    else:
        own_gu = [
            pltpu.make_async_copy(gate_ref, w_gu.at[z, :, pl.ds(0, unit)], local_sem.at[0]),
            pltpu.make_async_copy(up_ref, w_gu.at[z, :, pl.ds(unit, unit)], local_sem.at[1]),
        ]
    if subs == 1:
        own_dn = pltpu.make_async_copy(dn_ref, w_dn.at[z, 0, :, :, pl.ds(0, unit)], local_sem.at[2])
    else:
        own_dn = pltpu.make_async_copy(dn_ref, w_dn.at[z, 0], local_sem.at[2])
    for copy in own_gu:
        copy.start()
    own_dn.start()

    barrier = pltpu.get_barrier_semaphore()
    for s in range(1, ep):
        pl.semaphore_signal(
            barrier, inc=1, device_id={"ep": (me + s) % ep}, device_id_type=MESH
        )
    for s in range(1, tp):
        pl.semaphore_signal(
            barrier, inc=1, device_id={"tp": (mine + s) % tp}, device_id_type=MESH
        )
    pl.semaphore_wait(barrier, ep + tp - 2)

    def on_line(at):
        return (at >= 0) & (at <= chips - 1)

    def wants_gu(at):
        return (at >= 1) & (at <= chips - 2)

    def gu_part(src, j):
        return w_gu.at[src, pl.ds(j * deep, deep), pl.ds(0, lanes)]

    def gu_copy(src, j, way):
        return remote(
            gu_part(src, j),
            gu_part(src, j),
            gu_s.at[(1 - way) // 2, src, j],
            gu_r.at[src, j],
            {"tp": (z + way) * 2 + core},
        )

    def sg_copy(src, j):
        return remote(
            gu_part(src, j),
            w_gu.at[src, pl.ds(j * deep, deep), pl.ds(lanes, lanes)],
            sg_s.at[src, j],
            sg_r.at[src, j],
            {"tp": other},
        )

    def dn_part(src, c, which):
        if subs == 1:
            return w_dn.at[src, 0, c, :, pl.ds(which * unit, unit)]
        return w_dn.at[src, which, c]

    def dn_copy(src, c, way):
        return remote(
            dn_part(src, c, 0),
            dn_part(src, c, 0),
            dn_s.at[(1 - way) // 2, src, c],
            dn_r.at[src, c],
            {"tp": (z + way) * 2 + core},
        )

    def sd_copy(src, c):
        return remote(
            dn_part(src, c, 0), dn_part(src, c, 1), sd_s.at[src, c], sd_r.at[src, c], {"tp": other}
        )

    def start_own():
        for copy in own_gu:
            copy.wait()
        for way in (inward, -inward):

            @pl.when(wants_gu(z + way))
            def _(way=way):
                for j in range(PIECES):
                    gu_copy(z, j, way).start()

        own_dn.wait()
        for way in (inward, -inward):

            @pl.when(on_line(z + way))
            def _(way=way):
                for c in range(CHUNKS):
                    dn_copy(z, c, way).start()

        @pl.when(inner)
        def _():
            for j in range(PIECES):
                sg_copy(z, j).start()

        for c in range(CHUNKS):
            sd_copy(z, c).start()

    def source(k, near):
        return (z + k * inward, -inward) if near else (z - k * inward, inward)

    def pass_gu(k, near):
        src, way = source(k, near)

        @pl.when(inner & on_line(src))
        def _():
            for j in range(PIECES):
                gu_copy(src, j, way).wait_recv()
                pl.when(wants_gu(z + way))(lambda j=j: gu_copy(src, j, way).start())
                sg_copy(src, j).start()

    def ready_gu(src):
        for j in range(PIECES):
            sg_copy(src, j).wait_recv()

    def pass_dn(k, near, c):
        src, way = source(k, near)

        @pl.when(on_line(src))
        def _():
            dn_copy(src, c, way).wait_recv()
            pl.when(on_line(z + way))(lambda: dn_copy(src, c, way).start())
            sd_copy(src, c).start()

    def kv_copy(s):
        return remote(kv_ref, kv_all.at[s], kv_s.at[s], kv_r.at[s], {"ep": lax.rem(me + s, ep)})

    def send_kv():
        for s in range(1, ep):
            pl.when(me + s < ep)(lambda s=s: kv_copy(s).start())

    pl.when(inner)(start_own)
    pl.when(is_end)(send_kv)

    relative = ids_ref[...] - me
    relative = jnp.where(relative < 0, relative + ep, relative)
    table = (RANKS, local_rows)
    expert_row = lax.broadcasted_iota(jnp.int32, table, 0)
    named = jnp.zeros(table, F32)
    route = jnp.zeros(table, F32)
    for k in range(ids_ref.shape[0]):
        hit = expert_row == relative[k : k + 1, :]
        named = jnp.where(hit, 1.0, named)
        route = route + jnp.where(hit, group_ref[...] * gates_ref[k : k + 1, :], 0.0)
    square = (local_rows, local_rows)
    row_at = lax.broadcasted_iota(jnp.int32, square, 0)
    col_at = lax.broadcasted_iota(jnp.int32, square, 1)
    before = jnp.where(row_at < col_at, 1.0, 0.0).astype(BF16)
    rank = jnp.dot(named.astype(BF16), before, preferred_element_type=F32)
    rank_ref[0] = jnp.where(named > 0.5, rank, -1.0)
    tokens = tok_ref[...].astype(F32)
    nrm[0] = (
        tokens
        * lax.rsqrt(jnp.mean(tokens * tokens, axis=1, keepdims=True) + 1e-06)
        * norm_ref[...]
    ).astype(BF16)

    def guest_copies():
        target = {"tp": (z + inward) * 2 + core}
        return (
            remote(nrm.at[0], nrm.at[1], t_s.at[0], t_r.at[0], target),
            remote(rank_ref.at[0], rank_ref.at[1], t_s.at[1], t_r.at[1], target),
        )

    @pl.when(is_end)
    def _():
        for copy in guest_copies():
            copy.start()
        start_own()

    def x_copy(g, s):
        return remote(
            out_ref.at[g, s - 1],
            rows_x.at[pl.ds(g * half + s * cap, cap)],
            x_s.at[g, s],
            x_r.at[g, s],
            {"ep": lax.rem(me + s, ep)},
        )

    slot_row = lax.broadcasted_iota(jnp.int32, (cap, local_rows), 0).astype(F32)

    def place_of(g, s):
        return jnp.where(rank_ref[g, s : s + 1, :] == slot_row, 1.0, 0.0).astype(BF16)

    def dispatch(g):
        for s in list(range(1, ep)) + [0]:
            place = place_of(g, s)
            for n in range(CHUNKS):
                cols = slice(n * step, (n + 1) * step)
                picked = jnp.dot(place, nrm[g, :, cols], preferred_element_type=F32).astype(BF16)
                if s:
                    out_ref[g, s - 1, :, cols] = picked
                else:
                    rows_x[g * half : g * half + cap, cols] = picked
            if s:
                x_copy(g, s).start()

    pl.when(inner)(lambda: dispatch(0))

    tile = min(256, length)
    tiles = length // tile

    def attend(s):
        block = kv_ref if s == 0 else kv_all.at[s]

        def one(index, carry):
            h = index // tiles
            start = pl.multiple_of((index % tiles) * tile, tile)
            rows = pl.ds(start, tile)
            q = q_ref[h, rows, :]
            lane = lax.broadcasted_iota(jnp.int32, (tile, wide), 1)
            for m in range(2):
                pick = (lane < HEAD) if m == 0 else (lane >= HEAD)
                q_map = jnp.where(pick, q, jnp.zeros_like(q))
                scores = lax.dot_general(q_map, block[h, :, :wide], NT, preferred_element_type=F32)
                if s == 0:
                    row = start + lax.broadcasted_iota(jnp.int32, scores.shape, 0)
                    col = lax.broadcasted_iota(jnp.int32, scores.shape, 1)
                    scores = jnp.where(col <= row, scores, -1e30)
                    fresh = jnp.max(scores, axis=1, keepdims=True)
                else:
                    top = top_ref[m, h, rows, :]
                    fresh = jnp.maximum(top, jnp.max(scores, axis=1, keepdims=True))
                expo = jnp.exp(scores - fresh)
                total = jnp.sum(expo, axis=1, keepdims=True)
                value = jnp.dot(
                    expo.astype(BF16), block[h, :, wide:], preferred_element_type=F32
                )
                if s:
                    shrink = jnp.exp(top - fresh)
                    total = total + sum_ref[m, h, rows, :] * shrink
                    value = value + val_ref[m, h, rows, :] * shrink
                top_ref[m, h, rows, :] = fresh
                sum_ref[m, h, rows, :] = total
                val_ref[m, h, rows, :] = value
            return carry

        lax.fori_loop(0, heads * tiles, one, 0)

    def attend_later(s):
        @pl.when(me >= s)
        def _():
            kv_copy(s).wait_recv()
            attend(s)

    attend(0)

    for s in range(ep):
        place_ref[s] = place_of(0, s)
        column = jnp.sum(jnp.where(row_at == col_at, route[s : s + 1, :], 0.0), axis=1, keepdims=True)
        route_ref[:, s : s + 1] = column

    @pl.when(has_guest)
    def _():
        for copy in guest_copies():
            copy.wait_recv()
        dispatch(1)

    pl.when(inner)(send_kv)

    m_tile = half // 2

    def hidden_of(src, first, count):
        def one(t, carry):
            rows = pl.ds(pl.multiple_of(t * m_tile, m_tile), m_tile)
            product = jnp.dot(rows_x[rows, :], w_gu[src], preferred_element_type=F32)
            for i in range(2):
                gate = product[:, i * lanes : i * lanes + unit]
                value = gate / (1.0 + jnp.exp(-gate)) * product[:, i * lanes + unit : (i + 1) * lanes]
                if subs == 1:
                    hid[src, 0, rows, i * unit : (i + 1) * unit] = value.astype(BF16)
                else:
                    hid[src, i, rows, :] = value.astype(BF16)
            return carry

        lax.fori_loop(first, first + count, one, 0)

    def h_copy(src):
        return remote(
            hid.at[src, :, pl.ds(half, half)],
            hid.at[src, :, pl.ds(0, half)],
            h_s.at[src],
            h_r.at[src],
            {"tp": (z - inward) * 2 + core},
        )

    @pl.when(inner)
    def _():
        for s in range(1, ep):
            x_copy(0, s).wait_recv()
        ready_gu(z)
        hidden_of(z, 0, 2)

    pass_gu(1, True)

    @pl.when(inner)
    def _():
        ready_gu(z + inward)
        hidden_of(z + inward, 0, 2)

    pass_gu(1, False)
    for c in range(CHUNKS):
        pass_dn(1, True, c)

    @pl.when(has_guest)
    def _():
        for s in range(1, ep):
            x_copy(1, s).wait_recv()
        hidden_of(z, 2, 2)
        h_copy(z).start()
        hidden_of(z + inward, 2, 2)
        h_copy(z + inward).start()

    def use_gu(src):
        ready_gu(src)
        hidden_of(src, 0, 2)

        @pl.when(has_guest)
        def _():
            hidden_of(src, 2, 2)
            h_copy(src).start()

    pl.when(inner)(lambda: use_gu(z - inward))
    early = 1 + (ep - 1) // 3
    later = 1 + 2 * (ep - 1) // 3
    for s in range(1, early):
        attend_later(s)
    for c in range(CHUNKS):
        pass_dn(1, False, c)
    for s in range(early, later):
        attend_later(s)
    for k in range(2, chips):
        for near in (True, False):
            pass_gu(k, near)
            far = source(k, near)[0]
            pl.when(inner & on_line(far))(lambda far=far: use_gu(far))
    for s in range(later, ep):
        attend_later(s)

    def finish(index, carry):
        h = index // tiles
        rows = pl.ds(pl.multiple_of((index % tiles) * tile, tile), tile)
        diff = val_ref[0, h, rows, :] / sum_ref[0, h, rows, :] - mix_ref[h] * (
            val_ref[1, h, rows, :] / sum_ref[1, h, rows, :]
        )
        scaled = diff * lax.rsqrt(jnp.mean(diff * diff, axis=1, keepdims=True) + 1e-05)
        att[h, rows, :] = (scaled * gain_ref[...]).astype(BF16)
        return carry

    lax.fori_loop(0, heads * tiles, finish, 0)

    block = length // tp

    def project(t, carry):
        rows = pl.ds(pl.multiple_of(t * 2 * block, 2 * block), 2 * block)
        total = 0.0
        for h in range(heads):
            total = total + jnp.dot(att[h, rows, :], ow_ref[h], preferred_element_type=F32)
        part[0, t] = total[:block].astype(BF16)
        part[1, t] = total[block:].astype(BF16)
        return carry

    lax.fori_loop(0, chips, project, 0)
    pair_copy = remote(part.at[1 - core], pair, pr_s, pr_r, {"tp": other})
    pair_copy.start()
    pair_copy.wait_recv()

    def add_pair(t, carry):
        chip_sum[t] = (part[core, t].astype(F32) + pair[t].astype(F32)).astype(BF16)
        return carry

    lax.fori_loop(0, chips, add_pair, 0)

    def line_copy(side, t, first):
        return remote(
            chip_sum.at[t] if first else line_out.at[side, t],
            landed.at[side, t],
            rs_s.at[side, t],
            rs_r.at[side, t],
            {"tp": (z + 1 - 2 * side) * 2 + core},
        )

    def stage_each(k, do):
        for side in range(2):
            at = k if side == 0 else chips - 1 - k
            targets = range(chips - 1, k, -1) if side == 0 else range(chips - 1 - k)

            @pl.when(z == at)
            def _(side=side, targets=targets):
                for t in targets:
                    do(side, t, k == 0)

    def stage_send(side, t, first):
        copy = line_copy(side, t, first)
        if not first:
            copy.wait_recv()
            line_out[side, t] = (
                chip_sum[t].astype(F32) + landed[side, t].astype(F32)
            ).astype(BF16)
        copy.start()

    stage_each(0, stage_send)
    if chips > 2:
        stage_each(1, stage_send)

    @pl.when(is_end)
    def _():
        for src in range(chips):
            h_copy(src).wait_recv()

    def back_copy(c, s):
        return remote(
            back.at[c, pl.ds(s * cap, cap)],
            ret.at[c, s],
            b_s.at[c, s],
            b_r.at[c, s],
            {"ep": lax.rem(me + ep - s, ep)},
        )

    def down_of(c):
        def one(t, carry):
            rows = pl.ds(pl.multiple_of(t * m_tile, m_tile), m_tile)
            total = 0.0
            for src in range(chips):
                for i in range(subs):
                    total = total + lax.dot_general(
                        hid[src, i, rows, :], w_dn[src, i, c], NT, preferred_element_type=F32
                    )
            back[c, rows, :] = total.astype(BF16)
            return carry

        lax.fori_loop(0, 2, one, 0)

    def combine(c):
        total = 0.0
        for s in range(ep):
            if s == 0:
                block_rows = back[c, :cap, :]
            else:
                back_copy(c, s).wait_recv()
                block_rows = ret[c, s]
            picked = lax.dot_general(place_ref[s], block_rows, TN, preferred_element_type=F32)
            total = total + route_ref[:, s : s + 1] * picked
        routed_ref[:, c * step : (c + 1) * step] = total.astype(BF16)

    for c in range(CHUNKS):
        for k in range(2, chips):
            for near in (True, False):
                pass_dn(k, near, c)
        for src in range(chips):
            sd_copy(src, c).wait_recv()
        down_of(c)
        for s in range(1, ep):
            back_copy(c, s).start()
        if c == 1:
            for k in range(2, chips - 1):
                stage_each(k, stage_send)
        if c > 1:
            combine(c - 2)

    mixed_ref[...] = chip_sum[z]
    for side in range(2):

        @pl.when((z > 0) if side == 0 else (z < chips - 1))
        def _(side=side):
            line_copy(side, z, False).wait_recv()
            mixed_ref[...] = (
                mixed_ref[...].astype(F32) + landed[side, z].astype(F32)
            ).astype(BF16)

    for c in range(max(CHUNKS - 2, 0), CHUNKS):
        combine(c)

    for s in range(1, ep):
        pl.when(me + s < ep)(lambda s=s: kv_copy(s).wait_send())

        @pl.when(inner)
        def _(s=s):
            x_copy(0, s).wait_send()

        @pl.when(has_guest)
        def _(s=s):
            x_copy(1, s).wait_send()

    @pl.when(is_end)
    def _():
        for copy in guest_copies():
            copy.wait_send()

    @pl.when(has_guest)
    def _():
        for src in range(chips):
            h_copy(src).wait_send()

    for k in range(chips):
        for near in (True, False):
            src, way = source(k, near)

            @pl.when(on_line(src))
            def _(k=k, near=near, src=src, way=way):
                @pl.when(wants_gu(z + way) & (inner | (k == 0)))
                def _():
                    for j in range(PIECES):
                        gu_copy(src, j, way).wait_send()

                @pl.when(on_line(z + way))
                def _():
                    for c in range(CHUNKS):
                        dn_copy(src, c, way).wait_send()

                if k or near:

                    @pl.when(inner)
                    def _():
                        for j in range(PIECES):
                            sg_copy(src, j).wait_send()

                    for c in range(CHUNKS):
                        sd_copy(src, c).wait_send()

    pair_copy.wait_send()
    for k in range(chips - 1):
        stage_each(k, lambda side, t, first: line_copy(side, t, first).wait_send())
    for c in range(CHUNKS):
        for s in range(1, ep):
            back_copy(c, s).wait_send()


def per_device(
    queries,
    keys,
    values,
    mixing,
    head_gain,
    out_weight,
    tokens_b,
    norm_gain,
    expert_ids,
    group_gate,
    expert_gate,
    gate_weight,
    up_weight,
    down_weight,
):
    ep = lax.axis_size("ep")
    tp = lax.axis_size("tp")
    chips = tp // 2
    length, heads, wide = queries.shape
    val = values.shape[2]
    local_rows, width = tokens_b.shape
    top_count = expert_ids.shape[1]
    unit = gate_weight.shape[2]
    assert gate_weight.shape[0] == 1 and wide == 2 * HEAD and chips >= 4 and ep <= RANKS
    capacity = 3 * local_rows * top_count // (2 * ep)
    cap = -(-capacity // 16) * 16
    step = width // CHUNKS

    scaled = (queries.astype(F32) * (1.0 / math.sqrt(HEAD))).astype(BF16).transpose(1, 0, 2)
    kv = jnp.concatenate([keys, values], axis=2).transpose(1, 0, 2)
    gate, up = gate_weight[0], up_weight[0]
    subs = 1
    if unit % 128:
        gate = jnp.concatenate([gate, up], axis=1)
        subs = 2
    half = ep * cap
    block = length // tp
    vmem = pl.BlockSpec(memory_space=pltpu.VMEM)
    anywhere = pl.BlockSpec(memory_space=pl.ANY)
    dma = pltpu.SemaphoreType.DMA
    return pl.pallas_call(
        functools.partial(kernel, ep, tp),
        out_shape=(
            jax.ShapeDtypeStruct((block, width), BF16),
            jax.ShapeDtypeStruct((local_rows, width), BF16),
        ),
        in_specs=[pl.BlockSpec(memory_space=pltpu.SMEM)] + [vmem] * 9 + [anywhere] * 3,
        out_specs=(vmem, vmem),
        scratch_shapes=[
            pltpu.VMEM((ep, heads, length, wide + val), BF16),
            pltpu.VMEM((chips, width, 4 * unit), BF16),
            pltpu.VMEM((chips, subs, CHUNKS, step, 2 * unit // subs), BF16),
            pltpu.VMEM((2 * half, width), BF16),
            pltpu.VMEM((2, ep - 1, cap, width), BF16),
            pltpu.VMEM((2, local_rows, width), BF16),
            pltpu.VMEM((2, RANKS, local_rows), F32),
            pltpu.VMEM((chips, subs, 2 * half, 2 * unit // subs), BF16),
            pltpu.VMEM((CHUNKS, half, step), BF16),
            pltpu.VMEM((CHUNKS, ep, cap, step), BF16),
            pltpu.VMEM((2, heads, length, 1), F32),
            pltpu.VMEM((2, heads, length, 1), F32),
            pltpu.VMEM((2, heads, length, val), F32),
            pltpu.VMEM((heads, length, val), BF16),
            pltpu.VMEM((2, chips, block, width), BF16),
            pltpu.VMEM((chips, block, width), BF16),
            pltpu.VMEM((chips, block, width), BF16),
            pltpu.VMEM((2, chips, block, width), BF16),
            pltpu.VMEM((2, chips, block, width), BF16),
            pltpu.VMEM((ep, cap, local_rows), BF16),
            pltpu.VMEM((local_rows, ep), F32),
            dma((3,)),
            dma((ep,)),
            dma((ep,)),
            dma((2,)),
            dma((2,)),
            dma((2, ep)),
            dma((2, ep)),
            dma((2, chips, PIECES)),
            dma((chips, PIECES)),
            dma((chips, PIECES)),
            dma((chips, PIECES)),
            dma((2, chips, CHUNKS)),
            dma((chips, CHUNKS)),
            dma((chips, CHUNKS)),
            dma((chips, CHUNKS)),
            dma((chips,)),
            dma((chips,)),
            dma,
            dma,
            dma((2, chips)),
            dma((2, chips)),
            dma((CHUNKS, ep)),
            dma((CHUNKS, ep)),
        ],
        compiler_params=pltpu.CompilerParams(
            collective_id=0, has_side_effects=True, vmem_limit_bytes=62 * 1024 * 1024
        ),
    )(
        mixing,
        scaled,
        kv,
        head_gain[None],
        out_weight,
        tokens_b,
        norm_gain[None],
        expert_ids.T,
        group_gate[None],
        expert_gate.T,
        gate,
        up,
        down_weight[0].reshape(CHUNKS, step, unit),
    )


def solution(mesh):
    placed = (
        P("ep", "tp", None),
        P("ep", "tp", None),
        P("ep", "tp", None),
        P("tp"),
        P(),
        P("tp", None, None),
        P(("ep", "tp"), None),
        P(),
        P(("ep", "tp"), None),
        P(("ep", "tp")),
        P(("ep", "tp"), None),
        P("ep", None, "tp"),
        P("ep", None, "tp"),
        P("ep", None, "tp"),
    )
    return jax.shard_map(
        per_device,
        mesh=mesh,
        in_specs=placed,
        out_specs=(P(("ep", "tp"), None), P(("ep", "tp"), None)),
        check_vma=False,
    )
```

time: 133 us -> 123 us (0.925)
  Pallas kernels: 123 us -> 116 us
  local copies, waits for them, and re-layouts: 6.4 us -> 3.51 us
    pallas_call x1, Pallas kernels: 123 us -> 116 us  [per_device(): pl.pallas_call(functools.partial(kernel, ep, tp), out_shape=(jax.ShapeDty...]
    unnamed x18 -> x10, local copies, waits for them, and re-layouts: 5.65 us -> 3.51 us
where the time goes in v1:
time: 123 us
  Pallas kernels  116 us (94%)
  local copies, waits for them, and re-layouts  3.51 us (3%)
  other arithmetic  2.6 us (2%)
    pallas_call x1, Pallas kernels, per_device(): pl.pallas_call(functools.partial(kernel, ep, tp), out_shape=(jax.ShapeDty...  116 us
    unnamed x10, local copies, waits for them, and re-layouts  3.51 us

profile of v1, /device:TPU:0, one launch (start us, length us, event | category | flops | bytes accessed | tf_op | source)
XLA Modules:
  0.0 122.6 jit_solution(2486717715516280672)
XLA Ops:
  0.6 0.0 copy-start.1
  0.6 1.7 %fusion.q_ref = bf16[2,512,128]{2,1,0:T(8,128)(2,1)} fusion(bf16[512,2,128]{2,1,0:T(2,128)(2,1)} %param.14), kind=kLoop, calls=%fused_computation.2 | loop fusion | flops 393216 | bytes 524288 | tf_op jit(solution)/shard_map/transpose | solution.py:673
  2.4 0.0 copy-done.1
  2.4 0.0 copy-start.2
  2.4 0.9 copy-done.2
  3.4 0.9 maximum_bitcast_fusion.kv_ref
  4.2 115.8 %shard_map.149 = (bf16[64,2048]{1,0:T(8,128)(2,1)}, bf16[128,2048]{1,0:T(8,128)(2,1)}) custom-call(f32[2]{0:T(128)} %mix_ref.1, bf16[2,512,128]{2,1,0:T(8,128)(2,1)} %fusion.q_ref, bf16[2,512,256]{2,1,0:T(8,128)(2,1)} %maximum_bitcast_fusion.kv_ref, f32[1,128]{1,0:T(1,128)} %bitcast.18, bf16[2,128,2048]{2,1,0:T(8,128)(2,1)} %ow_ref.1, ...), custom_call_target="tpu_custom_call" | custom-call | tf_op jit(solution)/shard_map/pallas_call | solution.py:685
  120.0 0.0 copy-start
  120.0 1.7 %copy.22 = bf16[64,2048]{1,0:T(8,128)(2,1)} copy(bf16[64,2048]{1,0:T(8,128)(2,1)} %get-tuple-element.4) | data formatting | bytes 524288
  121.8 0.0 copy-done
  121.8 0.8 copy.23
  (2 shorter events, 0.1 us)
Async XLA Ops:
  0.6 1.8 %copy-start.1 = (bf16[512,2,128]{2,1,0:T(2,128)(2,1)S(1)}, bf16[512,2,128]{2,1,0:T(2,128)(2,1)}, u32[]{:S(2)}) copy-start(bf16[512,2,128]{2,1,0:T(2,128)(2,1)} %param.15) | copy-start | bytes 786436
  2.4 1.0 copy-start.2
  120.0 1.7 %copy-start = (bf16[128,2048]{1,0:T(8,128)(2,1)S(1)}, bf16[128,2048]{1,0:T(8,128)(2,1)}, u32[]{:S(2)}) copy-start(bf16[128,2048]{1,0:T(8,128)(2,1)} %get-tuple-element.5) | copy-start | bytes 1572868

commit v2 on v1

--- a/solution.py
+++ b/solution.py
@@ -10,6 +10,7 @@
 
 HEAD = 64
 CHUNKS = 4
+QUARTER = CHUNKS // 4
 PIECES = 2
 RANKS = 16
 F32 = jnp.float32
@@ -23,20 +24,27 @@
     ep,
     tp,
     mix_ref,
-    q_ref,
-    kv_ref,
     gain_ref,
-    ow_ref,
-    tok_ref,
     norm_ref,
     ids_ref,
     group_ref,
     gates_ref,
+    q_in,
+    k_in,
+    v_in,
+    ow_in,
+    tok_in,
     gate_ref,
     up_ref,
     dn_ref,
     mixed_ref,
     routed_ref,
+    q_raw,
+    k_raw,
+    v_raw,
+    ow_ref,
+    tok_ref,
+    q_ref,
     kv_all,
     w_gu,
     w_dn,
@@ -90,6 +98,7 @@
     other = z * 2 + 1 - core
     inward = 1 - 2 * (z // (chips // 2))
     heads, length, wide = q_ref.shape
+    val = val_ref.shape[3]
     local_rows, width = tok_ref.shape
     half = rows_x.shape[0] // 2
     cap = half // ep
@@ -124,9 +133,13 @@
         own_dn = pltpu.make_async_copy(dn_ref, w_dn.at[z, 0, :, :, pl.ds(0, unit)], local_sem.at[2])
     else:
         own_dn = pltpu.make_async_copy(dn_ref, w_dn.at[z, 0], local_sem.at[2])
-    for copy in own_gu:
-        copy.start()
-    own_dn.start()
+    own_kv = [
+        pltpu.make_async_copy(k_in, k_raw, local_sem.at[3]),
+        pltpu.make_async_copy(v_in, v_raw, local_sem.at[4]),
+        pltpu.make_async_copy(q_in, q_raw, local_sem.at[5]),
+    ]
+    own_tok = pltpu.make_async_copy(tok_in, tok_ref, local_sem.at[6])
+    own_ow = pltpu.make_async_copy(ow_in, ow_ref, local_sem.at[7])
 
     barrier = pltpu.get_barrier_semaphore()
     for s in range(1, ep):
@@ -137,6 +150,8 @@
         pl.semaphore_signal(
             barrier, inc=1, device_id={"tp": (mine + s) % tp}, device_id_type=MESH
         )
+    for copy in [own_tok] + own_gu + own_kv + [own_dn, own_ow]:
+        copy.start()
     pl.semaphore_wait(barrier, ep + tp - 2)
 
     def on_line(at):
@@ -195,34 +210,39 @@
                 for j in range(PIECES):
                     gu_copy(z, j, way).start()
 
-        own_dn.wait()
-        for way in (inward, -inward):
-
-            @pl.when(on_line(z + way))
-            def _(way=way):
-                for c in range(CHUNKS):
-                    dn_copy(z, c, way).start()
-
         @pl.when(inner)
         def _():
             for j in range(PIECES):
                 sg_copy(z, j).start()
 
+        own_dn.wait()
+
+        @pl.when(is_end)
+        def _():
+            for c in range(CHUNKS):
+                dn_copy(z, c, inward).start()
+
+        @pl.when(inner)
+        def _():
+            for c in range(CHUNKS):
+                dn_copy(z, c, -inward).start()
+            for c in range(2 * QUARTER, CHUNKS):
+                dn_copy(z, c, inward).start()
+
         for c in range(CHUNKS):
             sd_copy(z, c).start()
 
     def source(k, near):
         return (z + k * inward, -inward) if near else (z - k * inward, inward)
 
-    def pass_gu(k, near):
+    def pass_gu(k, near, j):
         src, way = source(k, near)
 
         @pl.when(inner & on_line(src))
         def _():
-            for j in range(PIECES):
-                gu_copy(src, j, way).wait_recv()
-                pl.when(wants_gu(z + way))(lambda j=j: gu_copy(src, j, way).start())
-                sg_copy(src, j).start()
+            gu_copy(src, j, way).wait_recv()
+            pl.when(wants_gu(z + way))(lambda: gu_copy(src, j, way).start())
+            sg_copy(src, j).start()
 
     def ready_gu(src):
         for j in range(PIECES):
@@ -237,15 +257,63 @@
             pl.when(on_line(z + way))(lambda: dn_copy(src, c, way).start())
             sd_copy(src, c).start()
 
+    square_plane = ep == 4
+    mid_rows = length // 2
+
+    def kv_move(src, dst, sem, target):
+        return remote(src, dst, kv_s.at[sem], kv_r.at[sem], {"ep": target})
+
     def kv_copy(s):
-        return remote(kv_ref, kv_all.at[s], kv_s.at[s], kv_r.at[s], {"ep": lax.rem(me + s, ep)})
-
-    def send_kv():
-        for s in range(1, ep):
-            pl.when(me + s < ep)(lambda s=s: kv_copy(s).start())
+        return kv_move(kv_all.at[0], kv_all.at[s], s, lax.rem(me + s, ep))
+
+    def kv_half(s, i):
+        rows = pl.ds(i * mid_rows, mid_rows)
+        return kv_move(kv_all.at[s, :, rows], kv_all.at[3, :, rows], 3 + i, 3)
+
+    def kv_corner():
+        return kv_move(kv_all.at[2], kv_all.at[1], 1, 2)
+
+    if square_plane:
+        near_sends = [((me == 0) | (me == 2), 1), (me <= 1, 2)]
+        far_sends = [
+            (me == 1, lambda: kv_half(1, 0)),
+            (me == 2, lambda: kv_half(2, 1)),
+            (me == 3, kv_corner),
+        ]
+        early_blocks = [((me == 1) | (me == 3), 1), (me >= 2, 2)]
+        late_blocks = [(me >= 2, jnp.where(me == 2, 1, 3))]
+    else:
+        near_sends = [(me + s < ep, s) for s in range(1, ep - 1)]
+        far_sends = [(me + ep - 1 < ep, lambda: kv_copy(ep - 1))]
+        early_blocks = [(me >= s, s) for s in range(1, ep - 1)]
+        late_blocks = [(me >= ep - 1, ep - 1)]
+
+    def send_near():
+        for sends, s in near_sends:
+            pl.when(sends)(lambda s=s: kv_copy(s).start())
+
+    def receive_near():
+        for has, s in early_blocks:
+            pl.when(has)(lambda s=s: kv_copy(s).wait_recv())
+
+    def send_far():
+        for sends, copy in far_sends:
+            pl.when(sends)(lambda copy=copy: copy().start())
+
+    def receive_far():
+        if square_plane:
+            pl.when(me == 2)(lambda: kv_corner().wait_recv())
+
+            @pl.when(me == 3)
+            def _():
+                kv_half(1, 0).wait_recv()
+                kv_half(2, 1).wait_recv()
+
+        else:
+            pl.when(me >= ep - 1)(lambda: kv_copy(ep - 1).wait_recv())
 
     pl.when(inner)(start_own)
-    pl.when(is_end)(send_kv)
+    own_tok.wait()
 
     relative = ids_ref[...] - me
     relative = jnp.where(relative < 0, relative + ep, relative)
@@ -283,6 +351,31 @@
             copy.start()
         start_own()
 
+    for copy in own_kv:
+        copy.wait()
+    part_rows = min(128, length)
+
+    def lay_kv(t, carry):
+        rows = pl.ds(pl.multiple_of(t * part_rows, part_rows), part_rows)
+        k_flat = k_raw[rows].reshape(part_rows, heads * wide)
+        v_flat = v_raw[rows].reshape(part_rows, heads * val)
+        for h in range(heads):
+            kv_all[0, h, rows, :wide] = k_flat[:, h * wide : (h + 1) * wide]
+            kv_all[0, h, rows, wide:] = v_flat[:, h * val : (h + 1) * val]
+        return carry
+
+    def lay_q(t, carry):
+        rows = pl.ds(pl.multiple_of(t * part_rows, part_rows), part_rows)
+        q_flat = q_raw[rows].reshape(part_rows, heads * wide)
+        for h in range(heads):
+            q = q_flat[:, h * wide : (h + 1) * wide].astype(F32) * (1.0 / math.sqrt(HEAD))
+            q_ref[h, rows, :] = q.astype(BF16)
+        return carry
+
+    lax.fori_loop(0, length // part_rows, lay_kv, 0)
+    send_near()
+    lax.fori_loop(0, length // part_rows, lay_q, 0)
+
     def x_copy(g, s):
         return remote(
             out_ref.at[g, s - 1],
@@ -310,13 +403,11 @@
             if s:
                 x_copy(g, s).start()
 
-    pl.when(inner)(lambda: dispatch(0))
-
     tile = min(256, length)
     tiles = length // tile
 
-    def attend(s):
-        block = kv_ref if s == 0 else kv_all.at[s]
+    def attend(s, first=False):
+        block = kv_all.at[s]
 
         def one(index, carry):
             h = index // tiles
@@ -328,7 +419,7 @@
                 pick = (lane < HEAD) if m == 0 else (lane >= HEAD)
                 q_map = jnp.where(pick, q, jnp.zeros_like(q))
                 scores = lax.dot_general(q_map, block[h, :, :wide], NT, preferred_element_type=F32)
-                if s == 0:
+                if first:
                     row = start + lax.broadcasted_iota(jnp.int32, scores.shape, 0)
                     col = lax.broadcasted_iota(jnp.int32, scores.shape, 1)
                     scores = jnp.where(col <= row, scores, -1e30)
@@ -341,7 +432,7 @@
                 value = jnp.dot(
                     expo.astype(BF16), block[h, :, wide:], preferred_element_type=F32
                 )
-                if s:
+                if not first:
                     shrink = jnp.exp(top - fresh)
                     total = total + sum_ref[m, h, rows, :] * shrink
                     value = value + val_ref[m, h, rows, :] * shrink
@@ -352,26 +443,12 @@
 
         lax.fori_loop(0, heads * tiles, one, 0)
 
-    def attend_later(s):
-        @pl.when(me >= s)
-        def _():
-            kv_copy(s).wait_recv()
-            attend(s)
-
-    attend(0)
+    attend(0, True)
 
     for s in range(ep):
         place_ref[s] = place_of(0, s)
         column = jnp.sum(jnp.where(row_at == col_at, route[s : s + 1, :], 0.0), axis=1, keepdims=True)
         route_ref[:, s : s + 1] = column
-
-    @pl.when(has_guest)
-    def _():
-        for copy in guest_copies():
-            copy.wait_recv()
-        dispatch(1)
-
-    pl.when(inner)(send_kv)
 
     m_tile = half // 2
 
@@ -399,58 +476,61 @@
             {"tp": (z - inward) * 2 + core},
         )
 
+    @pl.when(has_guest)
+    def _():
+        for copy in guest_copies():
+            copy.wait_recv()
+        dispatch(1)
+
+    receive_near()
+    send_far()
+    pl.when(inner)(lambda: dispatch(0))
+    for has, s in early_blocks:
+        pl.when(has)(lambda s=s: attend(s))
+    for j in range(PIECES):
+        pass_gu(1, True, j)
+    for j in range(PIECES - 1):
+        pass_gu(1, False, j)
+
+    def pass_near(first, last):
+        for c in range(first * QUARTER, last * QUARTER):
+            pass_dn(1, True, c)
+
+    pass_near(2, 4)
+
     @pl.when(inner)
     def _():
-        for s in range(1, ep):
-            x_copy(0, s).wait_recv()
         ready_gu(z)
-        hidden_of(z, 0, 2)
-
-    pass_gu(1, True)
-
-    @pl.when(inner)
-    def _():
         ready_gu(z + inward)
-        hidden_of(z + inward, 0, 2)
-
-    pass_gu(1, False)
-    for c in range(CHUNKS):
-        pass_dn(1, True, c)
+
+    def guest_hidden(src):
+        hidden_of(src, 2, 2)
+        h_copy(src).start()
 
     @pl.when(has_guest)
     def _():
         for s in range(1, ep):
             x_copy(1, s).wait_recv()
-        hidden_of(z, 2, 2)
-        h_copy(z).start()
-        hidden_of(z + inward, 2, 2)
-        h_copy(z + inward).start()
-
-    def use_gu(src):
-        ready_gu(src)
-        hidden_of(src, 0, 2)
-
-        @pl.when(has_guest)
-        def _():
-            hidden_of(src, 2, 2)
-            h_copy(src).start()
-
-    pl.when(inner)(lambda: use_gu(z - inward))
-    early = 1 + (ep - 1) // 3
-    later = 1 + 2 * (ep - 1) // 3
-    for s in range(1, early):
-        attend_later(s)
-    for c in range(CHUNKS):
+        guest_hidden(z)
+        guest_hidden(z + inward)
+
+    pass_gu(1, False, PIECES - 1)
+
+    @pl.when(inner)
+    def _():
+        for c in range(QUARTER):
+            dn_copy(z, c, inward).start()
+        ready_gu(z - inward)
+        pl.when(has_guest)(lambda: guest_hidden(z - inward))
+
+    for c in range(2 * QUARTER):
+        if c >= QUARTER:
+            pl.when(inner)(lambda c=c: dn_copy(z, c, inward).start())
         pass_dn(1, False, c)
-    for s in range(early, later):
-        attend_later(s)
-    for k in range(2, chips):
-        for near in (True, False):
-            pass_gu(k, near)
-            far = source(k, near)[0]
-            pl.when(inner & on_line(far))(lambda far=far: use_gu(far))
-    for s in range(later, ep):
-        attend_later(s)
+
+    receive_far()
+    for has, s in late_blocks:
+        pl.when(has)(lambda s=s: attend(s))
 
     def finish(index, carry):
         h = index // tiles
@@ -475,6 +555,7 @@
         part[1, t] = total[block:].astype(BF16)
         return carry
 
+    own_ow.wait()
     lax.fori_loop(0, chips, project, 0)
     pair_copy = remote(part.at[1 - core], pair, pr_s, pr_r, {"tp": other})
     pair_copy.start()
@@ -515,13 +596,19 @@
         copy.start()
 
     stage_each(0, stage_send)
-    if chips > 2:
-        stage_each(1, stage_send)
-
-    @pl.when(is_end)
-    def _():
-        for src in range(chips):
-            h_copy(src).wait_recv()
+
+    for c in range(2 * QUARTER, CHUNKS):
+        pass_dn(1, False, c)
+    for k in range(2, chips):
+        for near in (True, False):
+            for j in range(PIECES):
+                pass_gu(k, near, j)
+            far = source(k, near)[0]
+
+            @pl.when(inner & on_line(far))
+            def _(far=far):
+                ready_gu(far)
+                pl.when(has_guest)(lambda: guest_hidden(far))
 
     def back_copy(c, s):
         return remote(
@@ -558,20 +645,60 @@
             total = total + route_ref[:, s : s + 1] * picked
         routed_ref[:, c * step : (c + 1) * step] = total.astype(BF16)
 
-    for c in range(CHUNKS):
+    def pass_far(c):
         for k in range(2, chips):
             for near in (True, False):
                 pass_dn(k, near, c)
+
+    def give_back(c):
         for src in range(chips):
             sd_copy(src, c).wait_recv()
         down_of(c)
         for s in range(1, ep):
             back_copy(c, s).start()
-        if c == 1:
+
+    def own_hidden(first, last):
+        lax.fori_loop(first, last, lambda src, carry: (hidden_of(src, 0, 2), carry)[1], 0)
+
+    @pl.when(inner)
+    def _():
+        pass_near(0, 1)
+        for s in range(1, ep):
+            x_copy(0, s).wait_recv()
+        own_hidden(0, chips // 2)
+        for c in range(QUARTER):
+            pass_far(c)
+        own_hidden(chips // 2, chips)
+        pass_near(1, 2)
+        for c in range(QUARTER):
+            give_back(c)
+        for c in range(QUARTER, 2 * QUARTER):
+            pass_far(c)
+            give_back(c)
+        stage_each(1, stage_send)
+        for c in range(2 * QUARTER, CHUNKS):
+            pass_far(c)
+            give_back(c)
+
+    @pl.when(is_end)
+    def _():
+        pass_near(0, 1)
+        for c in range(QUARTER):
+            pass_far(c)
+        for src in range(chips):
+            h_copy(src).wait_recv()
+        for c in range(QUARTER):
+            give_back(c)
+        pass_near(1, 2)
+        for c in range(QUARTER, CHUNKS):
+            pass_far(c)
+            give_back(c)
+
+    for c in range(CHUNKS):
+        if c == CHUNKS // 2:
             for k in range(2, chips - 1):
                 stage_each(k, stage_send)
-        if c > 1:
-            combine(c - 2)
+        combine(c)
 
     mixed_ref[...] = chip_sum[z]
     for side in range(2):
@@ -583,11 +710,11 @@
                 mixed_ref[...].astype(F32) + landed[side, z].astype(F32)
             ).astype(BF16)
 
-    for c in range(max(CHUNKS - 2, 0), CHUNKS):
-        combine(c)
-
+    for sends, s in near_sends:
+        pl.when(sends)(lambda s=s: kv_copy(s).wait_send())
+    for sends, copy in far_sends:
+        pl.when(sends)(lambda copy=copy: copy().wait_send())
     for s in range(1, ep):
-        pl.when(me + s < ep)(lambda s=s: kv_copy(s).wait_send())
 
         @pl.when(inner)
         def _(s=s):
@@ -670,8 +797,6 @@
     cap = -(-capacity // 16) * 16
     step = width // CHUNKS
 
-    scaled = (queries.astype(F32) * (1.0 / math.sqrt(HEAD))).astype(BF16).transpose(1, 0, 2)
-    kv = jnp.concatenate([keys, values], axis=2).transpose(1, 0, 2)
     gate, up = gate_weight[0], up_weight[0]
     subs = 1
     if unit % 128:
@@ -688,9 +813,15 @@
             jax.ShapeDtypeStruct((block, width), BF16),
             jax.ShapeDtypeStruct((local_rows, width), BF16),
         ),
-        in_specs=[pl.BlockSpec(memory_space=pltpu.SMEM)] + [vmem] * 9 + [anywhere] * 3,
+        in_specs=[pl.BlockSpec(memory_space=pltpu.SMEM)] + [vmem] * 5 + [anywhere] * 8,
         out_specs=(vmem, vmem),
         scratch_shapes=[
+            pltpu.VMEM((length, heads, wide), BF16),
+            pltpu.VMEM((length, heads, wide), BF16),
+            pltpu.VMEM((length, heads, val), BF16),
+            pltpu.VMEM((heads, val, width), BF16),
+            pltpu.VMEM((local_rows, width), BF16),
+            pltpu.VMEM((heads, length, wide), BF16),
             pltpu.VMEM((ep, heads, length, wide + val), BF16),
             pltpu.VMEM((chips, width, 4 * unit), BF16),
             pltpu.VMEM((chips, subs, CHUNKS, step, 2 * unit // subs), BF16),
@@ -712,9 +843,9 @@
             pltpu.VMEM((2, chips, block, width), BF16),
             pltpu.VMEM((ep, cap, local_rows), BF16),
             pltpu.VMEM((local_rows, ep), F32),
-            dma((3,)),
-            dma((ep,)),
-            dma((ep,)),
+            dma((8,)),
+            dma((ep + 1,)),
+            dma((ep + 1,)),
             dma((2,)),
             dma((2,)),
             dma((2, ep)),
@@ -741,15 +872,16 @@
         ),
     )(
         mixing,
-        scaled,
-        kv,
         head_gain[None],
-        out_weight,
-        tokens_b,
         norm_gain[None],
         expert_ids.T,
         group_gate[None],
         expert_gate.T,
+        queries,
+        keys,
+        values,
+        out_weight,
+        tokens_b,
         gate,
         up,
         down_weight[0].reshape(CHUNKS, step, unit),

time: 123 us -> 106 us (0.86)
  Pallas kernels: 116 us -> 102 us
  other arithmetic: 2.6 us -> 0 us
    pallas_call x1, Pallas kernels: 116 us -> 102 us  [per_device(): pl.pallas_call(functools.partial(kernel, ep, tp), out_shape=(jax.ShapeDty...]
    transpose x2 -> x0, other arithmetic: 2.6 us -> none  [the longest x1 1.75 us: per_device(): (queries.astype(F32) * (1.0 / math.sqrt(HEAD))).astype(BF16)]
    unnamed x10 -> x4, local copies, waits for them, and re-layouts: 3.51 us -> 2.52 us
where the time goes in v2:
time: 106 us
  Pallas kernels  102 us (96%)
  local copies, waits for them, and re-layouts  2.52 us (2%)
    pallas_call x1, Pallas kernels, per_device(): pl.pallas_call(functools.partial(kernel, ep, tp), out_shape=(jax.ShapeDty...  102 us
    unnamed x4, local copies, waits for them, and re-layouts  2.52 us

profile of v2, /device:TPU:0, one launch (start us, length us, event | category | flops | bytes accessed | tf_op | source)
XLA Modules:
  0.0 105.6 jit_solution(5743329377558493396)
XLA Ops:
  0.6 102.4 %shard_map.149 = (bf16[64,2048]{1,0:T(8,128)(2,1)}, bf16[128,2048]{1,0:T(8,128)(2,1)}) custom-call(f32[2]{0:T(128)} %mix_ref.1, f32[1,128]{1,0:T(1,128)} %bitcast.14, f32[1,2048]{1,0:T(1,128)} %bitcast.11, s32[2,128]{1,0:T(2,128)} %bitcast.12, f32[1,128]{1,0:T(1,128)} %bitcast.15, f32[2,128]{1,0:T(2,128)} %bitcast.13, bf16[512,2,128]{2,1,0:T(2,128)(2,1)} %q_in.1, ...), custom_call_target="tpu_custom_call" | custom-call | tf_op jit(solution)/shard_map/pallas_call | solution.py:810
  103.0 0.0 copy-start
  103.0 1.7 %copy.18 = bf16[64,2048]{1,0:T(8,128)(2,1)} copy(bf16[64,2048]{1,0:T(8,128)(2,1)} %get-tuple-element.4) | data formatting | bytes 524288
  104.8 0.0 copy-done
  104.8 0.8 copy.19
Async XLA Ops:
  103.0 1.7 %copy-start = (bf16[128,2048]{1,0:T(8,128)(2,1)S(1)}, bf16[128,2048]{1,0:T(8,128)(2,1)}, u32[]{:S(2)}) copy-start(bf16[128,2048]{1,0:T(8,128)(2,1)} %get-tuple-element.5) | copy-start | bytes 1572868

commit v3 on v2

--- a/solution.py
+++ b/solution.py
@@ -9,8 +9,7 @@
 from jax.sharding import PartitionSpec as P
 
 HEAD = 64
-CHUNKS = 4
-QUARTER = CHUNKS // 4
+CHUNKS = 8
 PIECES = 2
 RANKS = 16
 F32 = jnp.float32
@@ -64,8 +63,7 @@
     chip_sum,
     landed,
     line_out,
-    place_ref,
-    route_ref,
+    take_ref,
     local_sem,
     kv_s,
     kv_r,
@@ -226,8 +224,6 @@
         def _():
             for c in range(CHUNKS):
                 dn_copy(z, c, -inward).start()
-            for c in range(2 * QUARTER, CHUNKS):
-                dn_copy(z, c, inward).start()
 
         for c in range(CHUNKS):
             sd_copy(z, c).start()
@@ -270,15 +266,21 @@
         rows = pl.ds(i * mid_rows, mid_rows)
         return kv_move(kv_all.at[s, :, rows], kv_all.at[3, :, rows], 3 + i, 3)
 
-    def kv_corner():
-        return kv_move(kv_all.at[2], kv_all.at[1], 1, 2)
+    def kv_corner(s, i):
+        rows = pl.ds(i * mid_rows, mid_rows)
+        return kv_move(kv_all.at[s, :, rows], kv_all.at[1, :, rows], 3 + i, 2)
+
+    def kv_lent():
+        rows = pl.ds(mid_rows, mid_rows)
+        return kv_move(kv_all.at[0, :, rows], kv_all.at[1, :, rows], 1, 0)
 
     if square_plane:
         near_sends = [((me == 0) | (me == 2), 1), (me <= 1, 2)]
         far_sends = [
             (me == 1, lambda: kv_half(1, 0)),
             (me == 2, lambda: kv_half(2, 1)),
-            (me == 3, kv_corner),
+            (me == 3, lambda: kv_corner(2, 0)),
+            (me == 0, lambda: kv_corner(1, 1)),
         ]
         early_blocks = [((me == 1) | (me == 3), 1), (me >= 2, 2)]
         late_blocks = [(me >= 2, jnp.where(me == 2, 1, 3))]
@@ -291,10 +293,14 @@
     def send_near():
         for sends, s in near_sends:
             pl.when(sends)(lambda s=s: kv_copy(s).start())
+        if square_plane:
+            pl.when(me == 1)(lambda: kv_lent().start())
 
     def receive_near():
         for has, s in early_blocks:
             pl.when(has)(lambda s=s: kv_copy(s).wait_recv())
+        if square_plane:
+            pl.when(me == 0)(lambda: kv_lent().wait_recv())
 
     def send_far():
         for sends, copy in far_sends:
@@ -302,7 +308,11 @@
 
     def receive_far():
         if square_plane:
-            pl.when(me == 2)(lambda: kv_corner().wait_recv())
+
+            @pl.when(me == 2)
+            def _():
+                kv_corner(2, 0).wait_recv()
+                kv_corner(1, 1).wait_recv()
 
             @pl.when(me == 3)
             def _():
@@ -445,10 +455,17 @@
 
     attend(0, True)
 
+    slot_at = lax.broadcasted_iota(jnp.int32, (local_rows, half), 1).astype(F32)
+    weight = jnp.zeros((local_rows, half), F32)
+    diagonal = row_at == col_at
     for s in range(ep):
-        place_ref[s] = place_of(0, s)
-        column = jnp.sum(jnp.where(row_at == col_at, route[s : s + 1, :], 0.0), axis=1, keepdims=True)
-        route_ref[:, s : s + 1] = column
+        rank_col = jnp.sum(jnp.where(diagonal, rank_ref[0, s : s + 1, :], 0.0), axis=1, keepdims=True)
+        route_col = jnp.sum(jnp.where(diagonal, route[s : s + 1, :], 0.0), axis=1, keepdims=True)
+        lane_of = jnp.where(rank_col >= 0.0, rank_col + float(s * cap), -1.0)
+        weight = jnp.where(slot_at == lane_of, route_col, weight)
+    upper = weight.astype(BF16)
+    take_ref[0] = upper
+    take_ref[1] = (weight - upper.astype(F32)).astype(BF16)
 
     m_tile = half // 2
 
@@ -476,62 +493,6 @@
             {"tp": (z - inward) * 2 + core},
         )
 
-    @pl.when(has_guest)
-    def _():
-        for copy in guest_copies():
-            copy.wait_recv()
-        dispatch(1)
-
-    receive_near()
-    send_far()
-    pl.when(inner)(lambda: dispatch(0))
-    for has, s in early_blocks:
-        pl.when(has)(lambda s=s: attend(s))
-    for j in range(PIECES):
-        pass_gu(1, True, j)
-    for j in range(PIECES - 1):
-        pass_gu(1, False, j)
-
-    def pass_near(first, last):
-        for c in range(first * QUARTER, last * QUARTER):
-            pass_dn(1, True, c)
-
-    pass_near(2, 4)
-
-    @pl.when(inner)
-    def _():
-        ready_gu(z)
-        ready_gu(z + inward)
-
-    def guest_hidden(src):
-        hidden_of(src, 2, 2)
-        h_copy(src).start()
-
-    @pl.when(has_guest)
-    def _():
-        for s in range(1, ep):
-            x_copy(1, s).wait_recv()
-        guest_hidden(z)
-        guest_hidden(z + inward)
-
-    pass_gu(1, False, PIECES - 1)
-
-    @pl.when(inner)
-    def _():
-        for c in range(QUARTER):
-            dn_copy(z, c, inward).start()
-        ready_gu(z - inward)
-        pl.when(has_guest)(lambda: guest_hidden(z - inward))
-
-    for c in range(2 * QUARTER):
-        if c >= QUARTER:
-            pl.when(inner)(lambda c=c: dn_copy(z, c, inward).start())
-        pass_dn(1, False, c)
-
-    receive_far()
-    for has, s in late_blocks:
-        pl.when(has)(lambda s=s: attend(s))
-
     def finish(index, carry):
         h = index // tiles
         rows = pl.ds(pl.multiple_of((index % tiles) * tile, tile), tile)
@@ -541,8 +502,6 @@
         scaled = diff * lax.rsqrt(jnp.mean(diff * diff, axis=1, keepdims=True) + 1e-05)
         att[h, rows, :] = (scaled * gain_ref[...]).astype(BF16)
         return carry
-
-    lax.fori_loop(0, heads * tiles, finish, 0)
 
     block = length // tp
 
@@ -555,17 +514,11 @@
         part[1, t] = total[block:].astype(BF16)
         return carry
 
-    own_ow.wait()
-    lax.fori_loop(0, chips, project, 0)
     pair_copy = remote(part.at[1 - core], pair, pr_s, pr_r, {"tp": other})
-    pair_copy.start()
-    pair_copy.wait_recv()
 
     def add_pair(t, carry):
         chip_sum[t] = (part[core, t].astype(F32) + pair[t].astype(F32)).astype(BF16)
         return carry
-
-    lax.fori_loop(0, chips, add_pair, 0)
 
     def line_copy(side, t, first):
         return remote(
@@ -595,60 +548,32 @@
             ).astype(BF16)
         copy.start()
 
-    stage_each(0, stage_send)
-
-    for c in range(2 * QUARTER, CHUNKS):
-        pass_dn(1, False, c)
-    for k in range(2, chips):
-        for near in (True, False):
-            for j in range(PIECES):
-                pass_gu(k, near, j)
-            far = source(k, near)[0]
-
-            @pl.when(inner & on_line(far))
-            def _(far=far):
-                ready_gu(far)
-                pl.when(has_guest)(lambda: guest_hidden(far))
-
     def back_copy(c, s):
         return remote(
             back.at[c, pl.ds(s * cap, cap)],
-            ret.at[c, s],
+            ret.at[c, pl.ds(s * cap, cap)],
             b_s.at[c, s],
             b_r.at[c, s],
             {"ep": lax.rem(me + ep - s, ep)},
         )
 
     def down_of(c):
-        def one(t, carry):
-            rows = pl.ds(pl.multiple_of(t * m_tile, m_tile), m_tile)
-            total = 0.0
-            for src in range(chips):
-                for i in range(subs):
-                    total = total + lax.dot_general(
-                        hid[src, i, rows, :], w_dn[src, i, c], NT, preferred_element_type=F32
-                    )
-            back[c, rows, :] = total.astype(BF16)
-            return carry
-
-        lax.fori_loop(0, 2, one, 0)
+        total = 0.0
+        for src in range(chips):
+            for i in range(subs):
+                total = total + lax.dot_general(
+                    hid[src, i, :half, :], w_dn[src, i, c], NT, preferred_element_type=F32
+                )
+        result = total.astype(BF16)
+        ret[c, :cap, :] = result[:cap]
+        back[c, cap:, :] = result[cap:]
 
     def combine(c):
-        total = 0.0
-        for s in range(ep):
-            if s == 0:
-                block_rows = back[c, :cap, :]
-            else:
-                back_copy(c, s).wait_recv()
-                block_rows = ret[c, s]
-            picked = lax.dot_general(place_ref[s], block_rows, TN, preferred_element_type=F32)
-            total = total + route_ref[:, s : s + 1] * picked
+        for s in range(1, ep):
+            back_copy(c, s).wait_recv()
+        total = jnp.dot(take_ref[0], ret[c], preferred_element_type=F32)
+        total = total + jnp.dot(take_ref[1], ret[c], preferred_element_type=F32)
         routed_ref[:, c * step : (c + 1) * step] = total.astype(BF16)
-
-    def pass_far(c):
-        for k in range(2, chips):
-            for near in (True, False):
-                pass_dn(k, near, c)
 
     def give_back(c):
         for src in range(chips):
@@ -660,38 +585,109 @@
     def own_hidden(first, last):
         lax.fori_loop(first, last, lambda src, carry: (hidden_of(src, 0, 2), carry)[1], 0)
 
+    def guest_hidden(src):
+        hidden_of(src, 2, 2)
+        h_copy(src).start()
+
+    def pass_rest(c):
+        for k in range(1, chips):
+            for near in (True, False):
+                if k > 1 or near:
+                    pass_dn(k, near, c)
+
+    def start_mixed():
+        lax.fori_loop(0, heads * tiles, finish, 0)
+        own_ow.wait()
+        lax.fori_loop(0, chips, project, 0)
+        pair_copy.start()
+
+    def chip_mixed():
+        pair_copy.wait_recv()
+        lax.fori_loop(0, chips, add_pair, 0)
+
+    def attend_far():
+        receive_far()
+        for has, s in late_blocks:
+            pl.when(has)(lambda s=s: attend(s))
+
+    @pl.when(has_guest)
+    def _():
+        for copy in guest_copies():
+            copy.wait_recv()
+        dispatch(1)
+
+    receive_near()
+    send_far()
+    for has, s in early_blocks:
+        pl.when(has)(lambda s=s: attend(s))
+
     @pl.when(inner)
     def _():
-        pass_near(0, 1)
+        for j in range(PIECES):
+            pass_gu(1, True, j)
+        for j in range(PIECES - 1):
+            pass_gu(1, False, j)
+        ready_gu(z)
+        ready_gu(z + inward)
+
+    @pl.when(has_guest)
+    def _():
+        for s in range(1, ep):
+            x_copy(1, s).wait_recv()
+        guest_hidden(z)
+        guest_hidden(z + inward)
+
+    @pl.when(inner)
+    def _():
+        dispatch(0)
+        pass_gu(1, False, PIECES - 1)
+        ready_gu(z - inward)
+        pl.when(has_guest)(lambda: guest_hidden(z - inward))
+        for c in range(CHUNKS):
+            if c == CHUNKS // 2:
+                attend_far()
+            dn_copy(z, c, inward).start()
+            pass_dn(1, False, c)
+        for k in range(2, chips):
+            for near in (True, False):
+                for j in range(PIECES):
+                    pass_gu(k, near, j)
+                far = source(k, near)[0]
+
+                @pl.when(on_line(far))
+                def _(far=far):
+                    ready_gu(far)
+                    pl.when(has_guest)(lambda: guest_hidden(far))
+
+        pass_rest(0)
+        start_mixed()
+        pass_rest(1)
         for s in range(1, ep):
             x_copy(0, s).wait_recv()
         own_hidden(0, chips // 2)
-        for c in range(QUARTER):
-            pass_far(c)
+        pass_rest(2)
         own_hidden(chips // 2, chips)
-        pass_near(1, 2)
-        for c in range(QUARTER):
-            give_back(c)
-        for c in range(QUARTER, 2 * QUARTER):
-            pass_far(c)
+        pass_rest(3)
+        chip_mixed()
+        for c in range(4):
             give_back(c)
         stage_each(1, stage_send)
-        for c in range(2 * QUARTER, CHUNKS):
-            pass_far(c)
+        for c in range(4, CHUNKS):
+            pass_rest(c)
             give_back(c)
 
     @pl.when(is_end)
     def _():
-        pass_near(0, 1)
-        for c in range(QUARTER):
-            pass_far(c)
+        attend_far()
+        start_mixed()
+        chip_mixed()
+        stage_each(0, stage_send)
+        pass_rest(0)
         for src in range(chips):
             h_copy(src).wait_recv()
-        for c in range(QUARTER):
-            give_back(c)
-        pass_near(1, 2)
-        for c in range(QUARTER, CHUNKS):
-            pass_far(c)
+        give_back(0)
+        for c in range(1, CHUNKS):
+            pass_rest(c)
             give_back(c)
 
     for c in range(CHUNKS):
@@ -712,6 +708,8 @@
 
     for sends, s in near_sends:
         pl.when(sends)(lambda s=s: kv_copy(s).wait_send())
+    if square_plane:
+        pl.when(me == 1)(lambda: kv_lent().wait_send())
     for sends, copy in far_sends:
         pl.when(sends)(lambda copy=copy: copy().wait_send())
     for s in range(1, ep):
@@ -810,8 +808,8 @@
     return pl.pallas_call(
         functools.partial(kernel, ep, tp),
         out_shape=(
-            jax.ShapeDtypeStruct((block, width), BF16),
-            jax.ShapeDtypeStruct((local_rows, width), BF16),
+            pltpu.VMEM((block, width), BF16),
+            pltpu.VMEM((local_rows, width), BF16),
         ),
         in_specs=[pl.BlockSpec(memory_space=pltpu.SMEM)] + [vmem] * 5 + [anywhere] * 8,
         out_specs=(vmem, vmem),
@@ -831,7 +829,7 @@
             pltpu.VMEM((2, RANKS, local_rows), F32),
             pltpu.VMEM((chips, subs, 2 * half, 2 * unit // subs), BF16),
             pltpu.VMEM((CHUNKS, half, step), BF16),
-            pltpu.VMEM((CHUNKS, ep, cap, step), BF16),
+            pltpu.VMEM((CHUNKS, half, step), BF16),
             pltpu.VMEM((2, heads, length, 1), F32),
             pltpu.VMEM((2, heads, length, 1), F32),
             pltpu.VMEM((2, heads, length, val), F32),
@@ -841,8 +839,7 @@
             pltpu.VMEM((chips, block, width), BF16),
             pltpu.VMEM((2, chips, block, width), BF16),
             pltpu.VMEM((2, chips, block, width), BF16),
-            pltpu.VMEM((ep, cap, local_rows), BF16),
-            pltpu.VMEM((local_rows, ep), F32),
+            pltpu.VMEM((2, local_rows, half), BF16),
             dma((8,)),
             dma((ep + 1,)),
             dma((ep + 1,)),

time: 106 us -> 100 us (0.943)
  Pallas kernels: 102 us -> 97.8 us
    pallas_call x1, Pallas kernels: 102 us -> 97.8 us  [per_device(): pl.pallas_call(functools.partial(kernel, ep, tp), out_shape=(pltpu.VMEM((...]
    unnamed x4 -> x2, local copies, waits for them, and re-layouts: 2.52 us -> 1.5 us
where the time goes in v3:
time: 100 us; the launch traced here: 99.9 us
  Pallas kernels  97.8 us (98%)
  local copies, waits for them, and re-layouts  1.5 us (2%)
    pallas_call x1, Pallas kernels, per_device(): pl.pallas_call(functools.partial(kernel, ep, tp), out_shape=(pltpu.VMEM((...  97.8 us

profile of v3, /device:TPU:0, one launch (start us, length us, event | category | flops | bytes accessed | tf_op | source)
XLA Modules:
  0.0 99.9 jit_solution(502818081786471967)
XLA Ops:
  0.6 97.8 %shard_map.149 = (bf16[64,2048]{1,0:T(8,128)(2,1)S(1)}, bf16[128,2048]{1,0:T(8,128)(2,1)S(1)}) custom-call(f32[2]{0:T(128)} %mix_ref.1, f32[1,128]{1,0:T(1,128)} %bitcast.14, f32[1,2048]{1,0:T(1,128)} %bitcast.11, s32[2,128]{1,0:T(2,128)} %bitcast.12, f32[1,128]{1,0:T(1,128)} %bitcast.15, f32[2,128]{1,0:T(2,128)} %bitcast.13, bf16[512,2,128]{2,1,0:T(2,128)(2,1)} %q_in.1, ...), custom_call_target="tpu_custom_call" | custom-call | tf_op jit(solution)/shard_map/pallas_call | solution.py:808
  98.4 0.7 copy.18
  99.1 0.8 copy.19

commit v4 on v3

--- a/solution.py
+++ b/solution.py
@@ -10,6 +10,7 @@
 
 HEAD = 64
 CHUNKS = 8
+LATE = 6
 PIECES = 2
 RANKS = 16
 F32 = jnp.float32
@@ -144,13 +145,22 @@
         pl.semaphore_signal(
             barrier, inc=1, device_id={"ep": (me + s) % ep}, device_id_type=MESH
         )
-    for s in range(1, tp):
-        pl.semaphore_signal(
-            barrier, inc=1, device_id={"tp": (mine + s) % tp}, device_id_type=MESH
-        )
+    pl.semaphore_signal(barrier, inc=1, device_id={"tp": other}, device_id_type=MESH)
+    for way in (-1, 1):
+
+        @pl.when((z + way >= 0) & (z + way <= chips - 1))
+        def _(way=way):
+            pl.semaphore_signal(
+                barrier,
+                inc=1,
+                device_id={"tp": (z + way) * 2 + core},
+                device_id_type=MESH,
+            )
+
     for copy in [own_tok] + own_gu + own_kv + [own_dn, own_ow]:
         copy.start()
-    pl.semaphore_wait(barrier, ep + tp - 2)
+    on_sides = (z + chips - 1) // chips + (2 * chips - 2 - z) // chips
+    pl.semaphore_wait(barrier, ep + on_sides)
 
     def on_line(at):
         return (at >= 0) & (at <= chips - 1)
@@ -165,7 +175,7 @@
         return remote(
             gu_part(src, j),
             gu_part(src, j),
-            gu_s.at[(1 - way) // 2, src, j],
+            gu_s.at[(1 - way) // 2, src],
             gu_r.at[src, j],
             {"tp": (z + way) * 2 + core},
         )
@@ -174,7 +184,7 @@
         return remote(
             gu_part(src, j),
             w_gu.at[src, pl.ds(j * deep, deep), pl.ds(lanes, lanes)],
-            sg_s.at[src, j],
+            sg_s.at[src],
             sg_r.at[src, j],
             {"tp": other},
         )
@@ -188,15 +198,37 @@
         return remote(
             dn_part(src, c, 0),
             dn_part(src, c, 0),
-            dn_s.at[(1 - way) // 2, src, c],
+            dn_s.at[(1 - way) // 2, src],
             dn_r.at[src, c],
             {"tp": (z + way) * 2 + core},
         )
 
     def sd_copy(src, c):
         return remote(
-            dn_part(src, c, 0), dn_part(src, c, 1), sd_s.at[src, c], sd_r.at[src, c], {"tp": other}
-        )
+            dn_part(src, c, 0), dn_part(src, c, 1), sd_s.at[src], sd_r.at[c], {"tp": other}
+        )
+
+    def gu_sent(src, way):
+        whole = w_gu.at[src, :, pl.ds(0, lanes)]
+        sem = gu_s.at[(1 - way) // 2, src]
+        remote(whole, whole, sem, gu_r.at[src, 0], {"tp": other}).wait_send()
+
+    def sg_sent(src):
+        whole = w_gu.at[src, :, pl.ds(0, lanes)]
+        remote(whole, whole, sg_s.at[src], sg_r.at[src, 0], {"tp": other}).wait_send()
+
+    def dn_whole(src):
+        if subs == 1:
+            return w_dn.at[src, 0, :, :, pl.ds(0, unit)]
+        return w_dn.at[src, 0]
+
+    def dn_sent(src, way):
+        whole, sem = dn_whole(src), dn_s.at[(1 - way) // 2, src]
+        remote(whole, whole, sem, dn_r.at[src, 0], {"tp": other}).wait_send()
+
+    def sd_sent(src):
+        whole = dn_whole(src)
+        remote(whole, whole, sd_s.at[src], sd_r.at[0], {"tp": other}).wait_send()
 
     def start_own():
         for copy in own_gu:
@@ -224,6 +256,8 @@
         def _():
             for c in range(CHUNKS):
                 dn_copy(z, c, -inward).start()
+            for c in range(LATE, CHUNKS):
+                dn_copy(z, c, inward).start()
 
         for c in range(CHUNKS):
             sd_copy(z, c).start()
@@ -552,8 +586,8 @@
         return remote(
             back.at[c, pl.ds(s * cap, cap)],
             ret.at[c, pl.ds(s * cap, cap)],
-            b_s.at[c, s],
-            b_r.at[c, s],
+            b_s.at[s],
+            b_r.at[c],
             {"ep": lax.rem(me + ep - s, ep)},
         )
 
@@ -569,15 +603,17 @@
         back[c, cap:, :] = result[cap:]
 
     def combine(c):
-        for s in range(1, ep):
-            back_copy(c, s).wait_recv()
+        slots = pl.ds(cap, half - cap)
+        remote(
+            back.at[c, slots], ret.at[c, slots], b_s.at[0], b_r.at[c], {"tp": other}
+        ).wait_recv()
         total = jnp.dot(take_ref[0], ret[c], preferred_element_type=F32)
         total = total + jnp.dot(take_ref[1], ret[c], preferred_element_type=F32)
         routed_ref[:, c * step : (c + 1) * step] = total.astype(BF16)
 
     def give_back(c):
-        for src in range(chips):
-            sd_copy(src, c).wait_recv()
+        whole = w_dn.at[:, 0, c, :, pl.ds(unit, unit)] if subs == 1 else w_dn.at[:, 1, c]
+        remote(whole, whole, sd_s.at[0], sd_r.at[c], {"tp": other}).wait_recv()
         down_of(c)
         for s in range(1, ep):
             back_copy(c, s).start()
@@ -589,8 +625,8 @@
         hidden_of(src, 2, 2)
         h_copy(src).start()
 
-    def pass_rest(c):
-        for k in range(1, chips):
+    def pass_rest(c, first=1):
+        for k in range(first, chips):
             for near in (True, False):
                 if k > 1 or near:
                     pass_dn(k, near, c)
@@ -627,6 +663,8 @@
             pass_gu(1, True, j)
         for j in range(PIECES - 1):
             pass_gu(1, False, j)
+        for c in range(LATE, CHUNKS):
+            pass_dn(1, True, c)
         ready_gu(z)
         ready_gu(z + inward)
 
@@ -646,7 +684,8 @@
         for c in range(CHUNKS):
             if c == CHUNKS // 2:
                 attend_far()
-            dn_copy(z, c, inward).start()
+            if c < LATE:
+                dn_copy(z, c, inward).start()
             pass_dn(1, False, c)
         for k in range(2, chips):
             for near in (True, False):
@@ -673,7 +712,7 @@
             give_back(c)
         stage_each(1, stage_send)
         for c in range(4, CHUNKS):
-            pass_rest(c)
+            pass_rest(c, 1 if c < LATE else 2)
             give_back(c)
 
     @pl.when(is_end)
@@ -740,30 +779,28 @@
             def _(k=k, near=near, src=src, way=way):
                 @pl.when(wants_gu(z + way) & (inner | (k == 0)))
                 def _():
-                    for j in range(PIECES):
-                        gu_copy(src, j, way).wait_send()
+                    gu_sent(src, way)
 
                 @pl.when(on_line(z + way))
                 def _():
-                    for c in range(CHUNKS):
-                        dn_copy(src, c, way).wait_send()
+                    dn_sent(src, way)
 
                 if k or near:
 
                     @pl.when(inner)
                     def _():
-                        for j in range(PIECES):
-                            sg_copy(src, j).wait_send()
-
-                    for c in range(CHUNKS):
-                        sd_copy(src, c).wait_send()
+                        sg_sent(src)
+
+                    sd_sent(src)
 
     pair_copy.wait_send()
     for k in range(chips - 1):
         stage_each(k, lambda side, t, first: line_copy(side, t, first).wait_send())
-    for c in range(CHUNKS):
-        for s in range(1, ep):
-            back_copy(c, s).wait_send()
+    for s in range(1, ep):
+        slots = pl.ds(s * cap, cap)
+        remote(
+            back.at[:, slots], ret.at[:, slots], b_s.at[s], b_r.at[0], {"tp": other}
+        ).wait_send()
 
 
 def per_device(
@@ -847,22 +884,22 @@
             dma((2,)),
             dma((2, ep)),
             dma((2, ep)),
-            dma((2, chips, PIECES)),
+            dma((2, chips)),
             dma((chips, PIECES)),
+            dma((chips,)),
             dma((chips, PIECES)),
-            dma((chips, PIECES)),
-            dma((2, chips, CHUNKS)),
+            dma((2, chips)),
             dma((chips, CHUNKS)),
-            dma((chips, CHUNKS)),
-            dma((chips, CHUNKS)),
+            dma((chips,)),
+            dma((CHUNKS,)),
             dma((chips,)),
             dma((chips,)),
             dma,
             dma,
             dma((2, chips)),
             dma((2, chips)),
-            dma((CHUNKS, ep)),
-            dma((CHUNKS, ep)),
+            dma((ep,)),
+            dma((CHUNKS,)),
         ],
         compiler_params=pltpu.CompilerParams(
             collective_id=0, has_side_effects=True, vmem_limit_bytes=62 * 1024 * 1024

time: 100 us -> 97.3 us (0.973)
  Pallas kernels: 97.8 us -> 95 us
    pallas_call x1, Pallas kernels: 97.8 us -> 95 us  [per_device(): pl.pallas_call(functools.partial(kernel, ep, tp), out_shape=(pltpu.VMEM((...]
where the time goes in v4:
time: 97.3 us; the launch traced here: 97.2 us
  Pallas kernels  95 us (98%)
  local copies, waits for them, and re-layouts  1.5 us (2%)
    pallas_call x1, Pallas kernels, per_device(): pl.pallas_call(functools.partial(kernel, ep, tp), out_shape=(pltpu.VMEM((...  95 us

profile of v4, /device:TPU:0, one launch (start us, length us, event | category | flops | bytes accessed | tf_op | source)
XLA Modules:
  0.0 97.2 jit_solution(5225044002141443637)
XLA Ops:
  0.6 95.0 %shard_map.149 = (bf16[64,2048]{1,0:T(8,128)(2,1)S(1)}, bf16[128,2048]{1,0:T(8,128)(2,1)S(1)}) custom-call(f32[2]{0:T(128)} %mix_ref.1, f32[1,128]{1,0:T(1,128)} %bitcast.14, f32[1,2048]{1,0:T(1,128)} %bitcast.11, s32[2,128]{1,0:T(2,128)} %bitcast.12, f32[1,128]{1,0:T(1,128)} %bitcast.15, f32[2,128]{1,0:T(2,128)} %bitcast.13, bf16[512,2,128]{2,1,0:T(2,128)(2,1)} %q_in.1, ...), custom_call_target="tpu_custom_call" | custom-call | tf_op jit(solution)/shard_map/pallas_call | solution.py:845
  95.7 0.7 copy.18
  96.4 0.8 copy.19

commit v5 on v4

--- a/solution.py
+++ b/solution.py
@@ -424,10 +424,14 @@
         return remote(
             out_ref.at[g, s - 1],
             rows_x.at[pl.ds(g * half + s * cap, cap)],
-            x_s.at[g, s],
-            x_r.at[g, s],
+            x_s.at[g],
+            x_r.at[g],
             {"ep": lax.rem(me + s, ep)},
         )
+
+    def x_whole(g):
+        whole = rows_x.at[pl.ds(g * half + cap, half - cap)]
+        return remote(whole, whole, x_s.at[g], x_r.at[g], {"tp": other})
 
     slot_row = lax.broadcasted_iota(jnp.int32, (cap, local_rows), 0).astype(F32)
 
@@ -522,8 +526,8 @@
         return remote(
             hid.at[src, :, pl.ds(half, half)],
             hid.at[src, :, pl.ds(0, half)],
-            h_s.at[src],
-            h_r.at[src],
+            h_s,
+            h_r,
             {"tp": (z - inward) * 2 + core},
         )
 
@@ -652,6 +656,10 @@
             copy.wait_recv()
         dispatch(1)
 
+    def h_whole():
+        whole = hid.at[:, :, pl.ds(0, half)]
+        return remote(whole, whole, h_s, h_r, {"tp": other})
+
     receive_near()
     send_far()
     for has, s in early_blocks:
@@ -670,8 +678,7 @@
 
     @pl.when(has_guest)
     def _():
-        for s in range(1, ep):
-            x_copy(1, s).wait_recv()
+        x_whole(1).wait_recv()
         guest_hidden(z)
         guest_hidden(z + inward)
 
@@ -701,8 +708,7 @@
         pass_rest(0)
         start_mixed()
         pass_rest(1)
-        for s in range(1, ep):
-            x_copy(0, s).wait_recv()
+        x_whole(0).wait_recv()
         own_hidden(0, chips // 2)
         pass_rest(2)
         own_hidden(chips // 2, chips)
@@ -722,8 +728,7 @@
         chip_mixed()
         stage_each(0, stage_send)
         pass_rest(0)
-        for src in range(chips):
-            h_copy(src).wait_recv()
+        h_whole().wait_recv()
         give_back(0)
         for c in range(1, CHUNKS):
             pass_rest(c)
@@ -751,15 +756,8 @@
         pl.when(me == 1)(lambda: kv_lent().wait_send())
     for sends, copy in far_sends:
         pl.when(sends)(lambda copy=copy: copy().wait_send())
-    for s in range(1, ep):
-
-        @pl.when(inner)
-        def _(s=s):
-            x_copy(0, s).wait_send()
-
-        @pl.when(has_guest)
-        def _(s=s):
-            x_copy(1, s).wait_send()
+    pl.when(inner)(lambda: x_whole(0).wait_send())
+    pl.when(has_guest)(lambda: x_whole(1).wait_send())
 
     @pl.when(is_end)
     def _():
@@ -768,8 +766,7 @@
 
     @pl.when(has_guest)
     def _():
-        for src in range(chips):
-            h_copy(src).wait_send()
+        h_whole().wait_send()
 
     for k in range(chips):
         for near in (True, False):
@@ -882,8 +879,8 @@
             dma((ep + 1,)),
             dma((2,)),
             dma((2,)),
-            dma((2, ep)),
-            dma((2, ep)),
+            dma((2,)),
+            dma((2,)),
             dma((2, chips)),
             dma((chips, PIECES)),
             dma((chips,)),
@@ -892,8 +889,8 @@
             dma((chips, CHUNKS)),
             dma((chips,)),
             dma((CHUNKS,)),
-            dma((chips,)),
-            dma((chips,)),
+            dma,
+            dma,
             dma,
             dma,
             dma((2, chips)),

time: 97.3 us -> 97.2 us (level)
  no operation moved by 1% of the time
where the time goes in v5:
time: 97.2 us; the launch traced here: 97 us
  Pallas kernels  94.9 us (98%)
  local copies, waits for them, and re-layouts  1.5 us (2%)
    pallas_call x1, Pallas kernels, per_device(): pl.pallas_call(functools.partial(kernel, ep, tp), out_shape=(pltpu.VMEM((...  94.9 us

profile of v5, /device:TPU:0, one launch (start us, length us, event | category | flops | bytes accessed | tf_op | source)
XLA Modules:
  0.0 97.0 jit_solution(8206951252767592486)
XLA Ops:
  0.6 94.9 %shard_map.149 = (bf16[64,2048]{1,0:T(8,128)(2,1)S(1)}, bf16[128,2048]{1,0:T(8,128)(2,1)S(1)}) custom-call(f32[2]{0:T(128)} %mix_ref.1, f32[1,128]{1,0:T(1,128)} %bitcast.14, f32[1,2048]{1,0:T(1,128)} %bitcast.11, s32[2,128]{1,0:T(2,128)} %bitcast.12, f32[1,128]{1,0:T(1,128)} %bitcast.15, f32[2,128]{1,0:T(2,128)} %bitcast.13, bf16[512,2,128]{2,1,0:T(2,128)(2,1)} %q_in.1, ...), custom_call_target="tpu_custom_call" | custom-call | tf_op jit(solution)/shard_map/pallas_call | solution.py:842
  95.5 0.7 copy.18
  96.2 0.8 copy.19
